TPU v7x, 256 devices: a whole 4x4x8 slice. The times are simulated.
256 devices in a mesh: sp: 32 (over z, x), tp: 8 (over y, core).
Axes of the slice: x: 4, y: 4, z: 8, core: 2. Of those that a mesh axis runs over, the one named last changes fastest.
Arguments:
- tokens: bfloat16 [8192, 1024], P(('sp', 'tp')), may hold values from -6 to 6
- doc_ids: int32 [8192], P('sp'), may hold values from 0 to 31, never falling along the last dimension, each value on 1 to 4608 neighbouring positions
- down_query: bfloat16 [1024, 256], P('sp'), may hold values from -0.1875 to 0.1875
- down_key: bfloat16 [1024, 256], P('sp'), may hold values from -0.1875 to 0.1875
- down_rotary: bfloat16 [1024, 32], P('sp'), may hold values from -0.1875 to 0.1875
- query_gain: float32 [256], replicated, may hold values from 0.1 to 1.9
- key_gain: float32 [256], replicated, may hold values from 0.1 to 1.9
- up_query: bfloat16 [256, 1536], P('sp', 'tp'), may hold values from -0.375 to 0.375
- up_key: bfloat16 [256, 1024], P('sp', 'tp'), may hold values from -0.375 to 0.375
- up_value: bfloat16 [256, 1024], P('sp', 'tp'), may hold values from -0.375 to 0.375
- output_weight: bfloat16 [1024, 1024], P('tp', 'sp'), may hold values from -0.1875 to 0.1875
- out_gain: float32 [1024], replicated, may hold values from 0.1 to 1.9
Outputs:
- mixed: bfloat16 [8192, 1024], P(('sp', 'tp'))
- log_sums: float32 [8192, 16], P('sp', 'tp')
Inputs may be any that keep to these rules, and one draw needn't show every extreme that they name: doc_ids never fall along the sequence and run from 0 to at most the number of devices along sp minus one; each document has 1 to 4608 positions, and one document has exactly that many.
All inputs are finite; a program needn't handle non-finite values.
Results may differ from a plain program's by a relative error of at most 0.02.
Values may be sent and summed in bfloat16 or wider, within the bound.
A program may use at most 64 MiB of HBM per device.

v0:
```python
import math

import jax
import jax.numpy as jnp
from jax import lax
from jax.sharding import Mesh
from jax.sharding import PartitionSpec as P

NOPE = 64
ROPE = 32
VDIM = 64
SP = ("sp_0", "sp_1")
TP = ("tp_0", "tp_1")
SP_TP = ("sp_0", "sp_1", "tp_0", "tp_1")


NEG_BIG = -1e30
THETA = 10000.0
EPS = 1e-06


def whole_of(value, axes, dim):
    for axis in reversed(axes):
        value = lax.all_gather(value, axis, axis=dim, tiled=True)
    return value


def folded(value, axes, dim, absorb, carry):
    everything = jax.tree.map(lambda part: whole_of(part, axes, dim), value)
    return absorb(carry, everything, jnp.int32(0))


def in_order(pieces, dim):
    shape = list(pieces.shape[1:])
    shape[dim] *= pieces.shape[0]
    return jnp.moveaxis(pieces, 0, dim).reshape(shape)


def gather_together(arrays, axis, dims):
    vector = jnp.concatenate([a.reshape(-1) for a in arrays])
    lines, at, outs = lax.all_gather(vector, axis), 0, []
    for a, dim in zip(arrays, dims):
        pieces = lines[:, at : at + a.size].reshape(-1, *a.shape)
        outs.append(in_order(pieces, dim))
        at += a.size
    return tuple(outs)


def over_axes(value, axes, dim, work):
    everything = whole_of(value, axes, dim)
    return work(everything, jnp.int32(0))


def own_rows_2(portion, extent, axis):
    count = extent * lax.axis_size(axis)
    sent = portion(jnp.int32(0), count).astype(jnp.bfloat16)
    return lax.psum_scatter(sent, axis, scatter_dimension=0, tiled=True).astype(jnp.float32)


def settle(quantity):
    return lax.optimization_barrier(quantity.astype(jnp.bfloat16))


def rms_gain(summed, gain_vector):
    widened = settle(summed).astype(jnp.float32)
    scaled = widened * lax.rsqrt(jnp.mean(widened * widened, axis=-1, keepdims=True) + EPS)
    return (scaled * gain_vector).astype(jnp.bfloat16)


def rotate(vectors, positions):
    half_width = vectors.shape[-1] // 2
    inverse = THETA ** (-jnp.arange(half_width, dtype=jnp.float32) / half_width)
    angles = positions.astype(jnp.float32)[:, None] * inverse[None, :]
    angles = angles.reshape((vectors.shape[0],) + (1,) * (vectors.ndim - 2) + (half_width,))
    cosine_part = jnp.cos(angles)
    sine_part = jnp.sin(angles)
    widened = vectors.astype(jnp.float32)
    front_half = widened[..., :half_width]
    back_half = widened[..., half_width:]
    return jnp.concatenate(
        [
            front_half * cosine_part - back_half * sine_part,
            back_half * cosine_part + front_half * sine_part,
        ],
        axis=-1,
    ).astype(jnp.bfloat16)


def over_blocks(carry, arrays, block_size, one_step):
    length = arrays[0].shape[0]
    if length == block_size:
        return one_step(carry, arrays)
    pieces_split = tuple(
        (array.reshape((length // block_size, block_size) + array.shape[1:]) for array in arrays)
    )

    def advance(carried, blocks):
        return (one_step(carried, blocks), None)

    carry, unused = lax.scan(advance, carry, pieces_split)
    return carry


def local(
    tokens,
    doc_ids,
    down_query,
    down_key,
    down_rotary,
    query_gain,
    key_gain,
    up_query,
    up_key,
    up_value,
    output_weight,
    out_gain,
):
    own_rows = tokens.shape[0]
    block_len = doc_ids.shape[0]
    local_heads = up_key.shape[1] // NOPE
    sp_base = lax.axis_index(SP) * block_len
    tp_first = lax.axis_index(TP) * own_rows
    row_pos = sp_base + tp_first + jnp.arange(own_rows, dtype=jnp.int32)
    score_scale = 1.0 / math.sqrt(NOPE + ROPE)

    def add_down(totals, pieces, offset):
        columns = lax.dynamic_slice_in_dim(tokens, offset, pieces[0].shape[0], 1)
        return tuple(
            (
                running + jnp.dot(columns, portion, preferred_element_type=jnp.float32)
                for running, portion in zip(totals, pieces)
            )
        )

    initial = tuple(
        (
            jnp.zeros((own_rows, weight.shape[1]), jnp.float32)
            for weight in (down_query, down_key, down_rotary)
        )
    )
    query_sum, latent_sum, rotary_sum = folded(
        (down_query, down_key, down_rotary), SP, 0, add_down, initial
    )
    query_latent = rms_gain(query_sum, query_gain)
    key_latent = rms_gain(latent_sum, key_gain)
    key_rot = rotate(settle(rotary_sum), row_pos)
    query_up, key_up, value_up = gather_together((up_query, up_key, up_value), SP, (0, 0, 0))

    def make_queries(portion, offset):
        length = portion.shape[0]
        positions = sp_base + offset + jnp.arange(length, dtype=jnp.int32)
        projected = settle(jnp.dot(portion, query_up, preferred_element_type=jnp.float32))
        projected = projected.reshape(length, local_heads, NOPE + ROPE)
        turned = rotate(projected[..., NOPE:], positions)
        joined_query = jnp.concatenate([projected[..., :NOPE], turned], axis=-1)
        return joined_query.reshape(length, local_heads * (NOPE + ROPE))

    queries = over_axes(query_latent, TP, 0, make_queries)
    queries = queries.reshape(block_len, local_heads, NOPE + ROPE)
    query_plain = queries[..., :NOPE]
    query_turned = queries[..., NOPE:]
    query_docs = doc_ids.astype(jnp.float32)

    def attend(carry, key_plain, key_turned, values, key_docs):
        top_score, weight_sum, accumulated = carry
        scores = jnp.einsum(
            "qhd,khd->hqk", query_plain, key_plain, preferred_element_type=jnp.float32
        )
        scores = scores + jnp.einsum(
            "qhr,kr->hqk", query_turned, key_turned, preferred_element_type=jnp.float32
        )
        scores = scores * score_scale
        same_doc = (query_docs[:, None] == key_docs[None, :])[None]
        new_top = jnp.maximum(top_score, jnp.max(jnp.where(same_doc, scores, NEG_BIG), axis=-1))
        weights = jnp.where(same_doc, jnp.exp(scores - new_top[..., None]), 0.0)
        rescale = jnp.exp(top_score - new_top)
        weight_sum = weight_sum * rescale + jnp.sum(weights, axis=-1)
        accumulated = accumulated * rescale.T[:, :, None] + jnp.einsum(
            "hqk,khv->qhv", weights.astype(jnp.bfloat16), values, preferred_element_type=jnp.float32
        )
        return (new_top, weight_sum, accumulated)

    def guarded(carry, key_plain, key_turned, values, key_docs):
        return attend(carry, key_plain, key_turned, values, key_docs)

    start_state = (
        jnp.full((local_heads, block_len), NEG_BIG, jnp.float32),
        jnp.zeros((local_heads, block_len), jnp.float32),
        jnp.zeros((block_len, local_heads, VDIM), jnp.float32),
    )
    latent_width = key_latent.shape[1]
    joined = jnp.concatenate([key_latent, key_rot], axis=1)

    def expand_rows(portion, offset):
        latent_rows = portion[:, :latent_width]
        turned_rows = portion[:, latent_width:]
        key_plain = jnp.dot(latent_rows, key_up, preferred_element_type=jnp.float32).astype(
            jnp.bfloat16
        )
        values = jnp.dot(latent_rows, value_up, preferred_element_type=jnp.float32).astype(
            jnp.bfloat16
        )
        return jnp.concatenate([key_plain, values, turned_rows], axis=1)

    expanded = over_axes(joined, TP, 0, expand_rows)

    def fold_expanded(carry, pieces, offset):

        def one_step(carried, blocks):
            rows_block, docs_rows = blocks
            length = rows_block.shape[0]
            plain_end = local_heads * NOPE
            value_end = local_heads * (NOPE + VDIM)
            key_plain = rows_block[:, :plain_end].reshape(length, local_heads, NOPE)
            values = rows_block[:, plain_end:value_end].reshape(length, local_heads, VDIM)
            turned_rows = rows_block[:, value_end:]
            return guarded(carried, key_plain, turned_rows, values, docs_rows.astype(jnp.float32))

        return over_blocks(carry, pieces, math.gcd(pieces[0].shape[0], block_len), one_step)

    carry = folded((expanded, doc_ids.astype(jnp.bfloat16)), SP, 0, fold_expanded, start_state)
    top_score, weight_sum, accumulated = carry
    log_sums = (top_score + jnp.log(weight_sum)).T
    attended = (accumulated / weight_sum.T[:, :, None]).astype(jnp.bfloat16)
    attended = attended.reshape(block_len, local_heads * VDIM)
    output_full = whole_of(output_weight, SP, 1)

    def project(offset, length):
        return jnp.dot(
            lax.dynamic_slice_in_dim(attended, offset, length, 0),
            output_full,
            preferred_element_type=jnp.float32,
        )

    summed = own_rows_2(project, own_rows, TP)
    return (rms_gain(summed, out_gain), log_sums)


def solution(mesh):
    finer = Mesh(mesh.devices.reshape(8, 4, 4, 2), ("sp_0", "sp_1", "tp_0", "tp_1"))
    return jax.shard_map(
        local,
        mesh=finer,
        in_specs=(
            P(SP_TP, None),
            P(SP),
            P(SP, None),
            P(SP, None),
            P(SP, None),
            P(),
            P(),
            P(SP, TP),
            P(SP, TP),
            P(SP, TP),
            P(TP, SP),
            P(),
        ),
        out_specs=(P(SP_TP, None), P(SP, TP)),
        check_vma=False,
    )
```

profile of v0, /device:TPU:1, one launch (start us, length us, event | category | flops | bytes accessed | tf_op | source)
XLA Modules:
  0.0 400.6 jit_solution(12858383854730480562)
XLA Ops:
  7.3 10.3 %all_gather.58 = bf16[128,32]{1,0:T(8,128)(2,1)S(1)} all-gather(bf16[32,32]{1,0:T(8,128)(2,1)} %param.18), channel_id=1, replica_groups=mesh['sp_0'=8,'sp_1'=4,'tp_0'=4,'tp_1'=2] {'sp_1'}, dimensions={0}, use_global_device_ids=true | all-gather | bytes 10240 | tf_op jit(solution)/shard_map/all_gather | solution.py:24
  17.6 22.0 %all_gather.59 = bf16[1024,32]{1,0:T(8,128)(2,1)S(1)} all-gather(bf16[128,32]{1,0:T(8,128)(2,1)S(1)} %all_gather.58), channel_id=1, replica_groups=mesh['sp_0'=8,'sp_1'=4,'tp_0'=4,'tp_1'=2] {'sp_0'}, dimensions={0}, use_global_device_ids=true | all-gather | bytes 73728 | tf_op jit(solution)/shard_map/all_gather | solution.py:24
  40.2 9.5 %all_gather.56 = bf16[128,256]{1,0:T(8,128)(2,1)S(1)} all-gather(bf16[32,256]{1,0:T(8,128)(2,1)} %param.17), channel_id=1, replica_groups=mesh['sp_0'=8,'sp_1'=4,'tp_0'=4,'tp_1'=2] {'sp_1'}, dimensions={0}, use_global_device_ids=true | all-gather | bytes 81920 | tf_op jit(solution)/shard_map/all_gather | solution.py:24
  49.7 19.2 %all_gather.57 = bf16[1024,256]{1,0:T(8,128)(2,1)S(1)} all-gather(bf16[128,256]{1,0:T(8,128)(2,1)S(1)} %all_gather.56), channel_id=1, replica_groups=mesh['sp_0'=8,'sp_1'=4,'tp_0'=4,'tp_1'=2] {'sp_0'}, dimensions={0}, use_global_device_ids=true | all-gather | bytes 589824 | tf_op jit(solution)/shard_map/all_gather | solution.py:24
  69.2 0.8 fusion.20
  70.0 20.1 %all_gather.60 = bf16[64,288]{1,0:T(8,128)(2,1)S(1)} all-gather(bf16[32,288]{1,0:T(8,128)(2,1)S(1)} %pad_maximum_fusion.2), channel_id=1, replica_groups=mesh['sp_0'=8,'sp_1'=4,'tp_0'=4,'tp_1'=2] {'tp_1'}, dimensions={0}, use_global_device_ids=true | all-gather | bytes 55296 | tf_op jit(solution)/shard_map/all_gather | solution.py:24
  90.1 10.1 %all_gather.61 = bf16[256,288]{1,0:T(8,128)(2,1)S(1)} all-gather(bf16[64,288]{1,0:T(8,128)(2,1)S(1)} %all_gather.60), channel_id=1, replica_groups=mesh['sp_0'=8,'sp_1'=4,'tp_0'=4,'tp_1'=2] {'tp_0'}, dimensions={0}, use_global_device_ids=true | all-gather | bytes 184320 | tf_op jit(solution)/shard_map/all_gather | solution.py:24
  100.2 0.8 reshape.157
  101.0 0.7 pad_maximum_fusion.3
  101.7 36.3 %all-gather.2 = bf16[32,1,3584]{2,1,0:T(2,128)(2,1)S(1)} all-gather(bf16[1,1,3584]{2,1,0:T(2,128)(2,1)S(1)} %reshape.167), channel_id=2, replica_groups=mesh['sp_0'=8,'sp_1'=4,'tp_0'=4,'tp_1'=2] {'sp_0','sp_1'}, dimensions={0}, use_global_device_ids=true | all-gather | bytes 236544 | tf_op jit(solution)/shard_map/all_gather | solution.py:41
  138.7 11.3 %all_gather.64 = bf16[1024,288]{0,1:T(8,128)(2,1)} all-gather(bf16[256,288]{0,1:T(8,128)(2,1)S(1)} %pad_maximum_fusion), channel_id=1, replica_groups=mesh['sp_0'=8,'sp_1'=4,'tp_0'=4,'tp_1'=2] {'sp_1'}, dimensions={0}, use_global_device_ids=true | all-gather | bytes 737280 | tf_op jit(solution)/shard_map/all_gather | solution.py:24
  150.2 9.5 %all_gather.66 = bf16[128,256]{1,0:T(8,128)(2,1)S(1)} all-gather(bf16[32,256]{1,0:T(8,128)(2,1)S(1)} %copy-done.1), channel_id=1, replica_groups=mesh['sp_0'=8,'sp_1'=4,'tp_0'=4,'tp_1'=2] {'sp_1'}, dimensions={0}, use_global_device_ids=true | all-gather | bytes 81920 | tf_op jit(solution)/shard_map/all_gather | solution.py:24
  159.6 19.5 %all_gather.67 = bf16[1024,256]{1,0:T(8,128)(2,1)S(1)} all-gather(bf16[128,256]{1,0:T(8,128)(2,1)S(1)} %all_gather.66), channel_id=1, replica_groups=mesh['sp_0'=8,'sp_1'=4,'tp_0'=4,'tp_1'=2] {'sp_0'}, dimensions={0}, use_global_device_ids=true | all-gather | bytes 589824 | tf_op jit(solution)/shard_map/all_gather | solution.py:24
  179.7 28.8 %all_gather.68 = bf16[64,256]{1,0:T(8,128)(2,1)S(1)} all-gather(bf16[32,256]{1,0:T(8,128)(2,1)S(1)} %fusion.23), channel_id=1, replica_groups=mesh['sp_0'=8,'sp_1'=4,'tp_0'=4,'tp_1'=2] {'tp_1'}, dimensions={0}, use_global_device_ids=true | all-gather | bytes 49152 | tf_op jit(solution)/shard_map/all_gather | solution.py:24
  208.6 10.3 %all_gather.69 = bf16[256,256]{1,0:T(8,128)(2,1)S(1)} all-gather(bf16[64,256]{1,0:T(8,128)(2,1)S(1)} %all_gather.68), channel_id=1, replica_groups=mesh['sp_0'=8,'sp_1'=4,'tp_0'=4,'tp_1'=2] {'tp_0'}, dimensions={0}, use_global_device_ids=true | all-gather | bytes 163840 | tf_op jit(solution)/shard_map/all_gather | solution.py:24
  219.2 7.5 %all-gather.1 = bf16[4,1,256]{2,1,0:T(2,128)(2,1)S(1)} all-gather(bf16[1,1,256]{2,1,0:T(2,128)(2,1)S(1)} %reshape.165), channel_id=1, replica_groups=mesh['sp_0'=8,'sp_1'=4,'tp_0'=4,'tp_1'=2] {'sp_1'}, dimensions={0}, use_global_device_ids=true | all-gather | bytes 2560 | tf_op jit(solution)/shard_map/all_gather | solution.py:24
  226.7 18.1 %all_gather.55 = bf16[8192]{0:T(1024)(128)(2,1)S(1)} all-gather(bf16[1024]{0:T(1024)(128)(2,1)S(1)} %bitcast.91), channel_id=1, replica_groups=mesh['sp_0'=8,'sp_1'=4,'tp_0'=4,'tp_1'=2] {'sp_0'}, dimensions={0}, use_global_device_ids=true | all-gather | bytes 18432 | tf_op jit(solution)/shard_map/all_gather | solution.py:24
  244.9 8.9 %all_gather.70 = bf16[128,128]{0,1:T(8,128)(2,1)S(1)} all-gather(bf16[128,32]{0,1:T(8,128)(2,1)S(1)} %copy-done.2), channel_id=1, replica_groups=mesh['sp_0'=8,'sp_1'=4,'tp_0'=4,'tp_1'=2] {'sp_1'}, dimensions={1}, use_global_device_ids=true | all-gather | bytes 40960 | tf_op jit(solution)/shard_map/all_gather | solution.py:24
  254.0 18.7 %all_gather.71 = bf16[128,1024]{0,1:T(8,128)(2,1)S(1)} all-gather(bf16[128,128]{0,1:T(8,128)(2,1)S(1)} %all_gather.70), channel_id=1, replica_groups=mesh['sp_0'=8,'sp_1'=4,'tp_0'=4,'tp_1'=2] {'sp_0'}, dimensions={1}, use_global_device_ids=true | all-gather | bytes 294912 | tf_op jit(solution)/shard_map/all_gather | solution.py:24
  272.7 5.1 %copy.36 = bf16[36,32,8,256]{3,2,0,1:T(8,128)(2,1)} copy(bf16[36,32,8,256]{3,2,1,0:T(8,128)(2,1)} %bitcast.83) | data formatting | bytes 9437184 | tf_op jit(solution)/shard_map/reshape | solution.py:94
  277.8 66.3 %while.15 = (s32[]{:T(128)}, f32[2,256]{1,0:T(2,128)S(1)}, f32[2,256]{1,0:T(2,128)S(1)}, f32[256,2,64]{0,2,1:T(8,128)S(1)}, f32[256]{0:T(256)S(1)}, /*index=5*/b...) while((s32[]{:T(128)}, f32[2,256]{1,0:T(2,128)S(1)}, ...), condition=%wide.region_5.6_spmd.clone, body=%wide.region_2.5_spmd.clone.sunk | while | flops 43420928 | bytes 3985025 | solution.py:100
  277.8 0.9 dynamic-slice_bitcast_fusion.2
  279.2 0.3 select_reduce_fusion.2
  279.9 0.9 dynamic-slice_bitcast_fusion.2
  281.2 0.3 select_reduce_fusion.2
  282.0 0.9 dynamic-slice_bitcast_fusion.2
  284.0 0.9 dynamic-slice_bitcast_fusion.2
  285.4 0.3 select_reduce_fusion.2
  286.1 0.9 dynamic-slice_bitcast_fusion.2
  287.4 0.3 select_reduce_fusion.2
  288.2 0.9 dynamic-slice_bitcast_fusion.2
  289.5 0.3 select_reduce_fusion.2
  290.2 0.9 dynamic-slice_bitcast_fusion.2
  291.6 0.3 select_reduce_fusion.2
  292.3 0.9 dynamic-slice_bitcast_fusion.2
  294.4 0.9 dynamic-slice_bitcast_fusion.2
  296.5 0.9 dynamic-slice_bitcast_fusion.2
  298.5 0.9 dynamic-slice_bitcast_fusion.2
  300.6 0.9 dynamic-slice_bitcast_fusion.2
  302.7 0.9 dynamic-slice_bitcast_fusion.2
  304.7 0.9 dynamic-slice_bitcast_fusion.2
  306.8 0.9 dynamic-slice_bitcast_fusion.2
  308.9 0.9 dynamic-slice_bitcast_fusion.2
  311.0 0.9 dynamic-slice_bitcast_fusion.2
  313.0 0.9 dynamic-slice_bitcast_fusion.2
  315.1 0.9 dynamic-slice_bitcast_fusion.2
  317.2 0.9 dynamic-slice_bitcast_fusion.2
  319.2 0.9 dynamic-slice_bitcast_fusion.2
  321.3 0.9 dynamic-slice_bitcast_fusion.2
  323.4 0.9 dynamic-slice_bitcast_fusion.2
  325.5 0.9 dynamic-slice_bitcast_fusion.2
  327.5 0.9 dynamic-slice_bitcast_fusion.2
  329.6 0.9 dynamic-slice_bitcast_fusion.2
  331.7 0.9 dynamic-slice_bitcast_fusion.2
  333.7 0.9 dynamic-slice_bitcast_fusion.2
  335.8 0.9 dynamic-slice_bitcast_fusion.2
  337.9 0.9 dynamic-slice_bitcast_fusion.2
  340.0 0.9 dynamic-slice_bitcast_fusion.2
  342.0 0.9 dynamic-slice_bitcast_fusion.2
  344.1 1.1 convolution_convert_fusion
  345.3 0.6 add_bitcast_fusion
  345.8 45.4 %reduce-scatter.2.cloned.1.call-done = bf16[32,1024]{1,0:T(8,128)(2,1)} async-done(((bf16[256,1024]{1,0:T(8,128)(2,1)}), bf16[32,1024]{1,0:T(8,128)(2,1)}) %reduce-scatter.2.cloned.1.call-update) | async-done | bytes 65552 | tf_op jit(solution)/shard_map/reduce_scatter | solution.py:57
  391.2 1.0 fusion.13
  392.2 1.6 fusion.15
  (375 shorter events, 35.2 us)
Async XLA Ops:
  7.2 32.5 %copy-start = (bf16[32,1024]{1,0:T(8,128)(2,1)S(1)}, bf16[32,1024]{1,0:T(8,128)(2,1)}, u32[]{:S(2)}) copy-start(bf16[32,1024]{1,0:T(8,128)(2,1)} %param.14) | copy-start | bytes 196612
  7.2 143.0 %copy-start.1 = (bf16[32,256]{1,0:T(8,128)(2,1)S(1)}, bf16[32,256]{1,0:T(8,128)(2,1)}, u32[]{:S(2)}) copy-start(bf16[32,256]{1,0:T(8,128)(2,1)} %param.16) | copy-start | bytes 49156
  7.2 172.5 %copy-start.4 = (f32[256]{0:T(256)S(1)}, f32[256]{0:T(256)}, u32[]{:S(2)}) copy-start(f32[256]{0:T(256)} %param.19) | copy-start | bytes 3076
  7.2 211.9 %copy-start.5 = (s32[256]{0:T(256)S(1)}, s32[256]{0:T(256)}, u32[]{:S(2)}) copy-start(s32[256]{0:T(256)} %param.15) | copy-start | bytes 3076
  7.2 237.6 %copy-start.2 = (bf16[128,32]{0,1:T(8,128)(2,1)S(1)}, bf16[128,32]{0,1:T(8,128)(2,1)}, u32[]{:S(2)}) copy-start(bf16[128,32]{0,1:T(8,128)(2,1)} %param.24) | copy-start | bytes 24580
  7.2 265.5 %all-gather.5.cloned.1.call-start = ((), (), s32[]{:S(2)}) async-start(), calls=%async_computation.1 | async-start | bytes 5308416 | tf_op jit(solution)/shard_map/all_gather | solution.py:24
  150.1 241.1 %reduce-scatter.2.cloned.1.call-start = ((), (), s32[]{:S(2)}) async-start(), calls=%async_computation.2 | async-start | bytes 589824 | tf_op jit(solution)/shard_map/reduce_scatter | solution.py:57
  277.8 114.4 %copy-start.3 = (f32[1024]{0:T(1024)S(1)}, f32[1024]{0:T(1024)}, u32[]{:S(2)}) copy-start(f32[1024]{0:T(1024)} %param.25) | copy-start | bytes 12292
Sparse Core Ops, SparseCore 0:
  150.2 75.6 all-gather.4
  345.4 45.7 reduce-scatter.1
where the time goes:
time: 403 us; the launch traced here: 401 us
  blocking collectives  260 us (65%)
  waiting for transfers between devices  45.4 us (11%)
  local copies, waits for them, and re-layouts  36.5 us (9%)
  matrix products  27.4 us (7%)
  between operations  14.4 us (4%)
  other arithmetic  14 us (3%)
    all_gather x15, blocking collectives, whole_of(): value = lax.all_gather(value, axis, axis=dim, tiled=True)  224 us
    reduce_scatter x1, waiting for transfers between devices, own_rows_2(): lax.psum_scatter(sent, axis, scatter_dimension=0, tiled=True)  45.4 us
    all_gather x1, blocking collectives, gather_together(): lines, at, outs = (lax.all_gather(vector, axis), 0, [])  36.3 us
    squeeze x32, local copies, waits for them, and re-layouts, over_blocks(): carry, unused = lax.scan(advance, carry, pieces_split)  29.6 us
    dot_general x32, matrix products, attend(): jnp.einsum('qhr,kr->hqk', query_turned, key_turned, preferred_element_typ...  8.78 us
    dot_general x32, matrix products, attend(): jnp.einsum('qhd,khd->hqk', query_plain, key_plain, preferred_element_type...  8.51 us
  transfers between devices with their start and end apart: 2, of which 1 were waited for; matrix products, arithmetic and copies ran while one was open for 0% of the time, Pallas kernels for 0%

commit v1 on v0

v1 whole, which is shorter than its diff:
```python
import functools
import math

import jax
import jax.numpy as jnp
from jax import lax
from jax.experimental import pallas as pl
from jax.experimental.pallas import tpu as pltpu
from jax.sharding import PartitionSpec as P

NOPE = 64
ROPE = 32
THETA = 10000.0
EPS = 1e-06
UNSEEN = -1e30
MASKED = -3e38
SCALE = 1.0 / math.sqrt(NOPE + ROPE)
SCALE_2 = SCALE * math.log2(math.e)
MESH = pl.DeviceIdType.MESH
F32 = jnp.float32
BF16 = jnp.bfloat16

STEPS = (0, 1, -1, 2, -2, 3, -3, 4)
SLOT_OF = {0: 0, 1: 1, -1: 2, 2: 3, -2: 4, 3: 5, -3: 6, 4: 7, -4: 7}
GROUPS = ((0, 4), (4, 4))


def slot8(r):
    late = r // 5
    return (1 - late) * (2 * r - 1 + (8 - r) // 8) + late * (16 - 2 * r)


def slot4(r):
    return 2 * r - r // 2 - 4 * (r // 3)


def nt(a, b):
    return lax.dot_general(a, b, (((1,), (1,)), ((), ())), preferred_element_type=F32)


def nn(a, b):
    return jnp.dot(a, b, preferred_element_type=F32)


def body(
    tok,
    wpiece,
    bundle,
    qdoc,
    kdoc,
    cos_q,
    sin_q,
    cos_k,
    sin_k,
    query_gain,
    key_gain,
    out_gain,
    mixed,
    log_sums,
    wbuf,
    bbuf,
    kbuf,
    qlbuf,
    w_down,
    w_rot,
    w_uq,
    w_uk,
    w_uv,
    w_out,
    kx_w,
    vt_w,
    qx,
    top,
    total,
    acc,
    partial,
    rsbuf,
    send_z,
    recv_z,
    send_2,
    recv_2,
    send_3,
    recv_3,
    send_p,
    recv_p,
    send_bz,
    recv_bz,
    send_bx,
    recv_bx,
    send_t,
    recv_t,
):
    sp = lax.axis_index("sp")
    tp = lax.axis_index("tp")
    z, x = sp // 4, sp % 4
    y, c = tp // 2, tp % 2

    def chip(dz=0, dx=0, dy=0, flip=False):
        core = 1 - c if flip else c
        return (((z + dz + 8) % 8) * 4 + (x + dx + 4) % 4, ((y + dy + 4) % 4) * 2 + core)

    def along_2(d):
        return chip(dx=(1 - c) * d, dy=c * d)

    def along_3(d):
        return chip(dx=c * d, dy=(1 - c) * d)

    tp_peers = [(dy, flip) for dy in (1, 3, 2, 0) for flip in (False, True) if (dy, flip) != (0, False)]

    barrier = pltpu.get_barrier_semaphore()
    peers = [chip(dz=d) for d in STEPS[1:]] + [chip(dx=1), chip(dx=-1)]
    peers += [chip(dy=dy, flip=flip) for dy, flip in tp_peers]
    for peer in peers:
        pl.semaphore_signal(barrier, inc=1, device_id=peer, device_id_type=MESH)
    pl.semaphore_wait(barrier, len(peers))

    started = []

    def push(src, dst, ssem, rsem, peer):
        copy = pltpu.make_async_remote_copy(
            src_ref=src, dst_ref=dst, send_sem=ssem, recv_sem=rsem, device_id=peer, device_id_type=MESH
        )
        copy.start()
        started.append(copy)

    def landed(dst, rsem):
        pltpu.make_async_remote_copy(
            src_ref=dst, dst_ref=dst, send_sem=rsem, recv_sem=rsem, device_id=chip(flip=True), device_id_type=MESH
        ).wait_recv()

    def spread(ids, buf, first):
        n2, n3 = 6 * ids, 24 * ids

        def go_z():
            for k in range(1, 8):
                slot = SLOT_OF[-STEPS[k]]
                push(first, buf.at[0, 0, 0, slot], send_z.at[ids, k - 1], recv_z.at[ids, slot - 1], chip(dz=STEPS[k]))

        def wait_z(g):
            lo, n = GROUPS[g]
            for k in range(max(lo, 1), lo + n):
                landed(buf.at[0, 0, 0, k], recv_z.at[ids, k - 1])

        def send_2nd(a_from, a_to, g, d):
            lo, n = GROUPS[g]
            i = n2 + (a_to - 1) * 2 + g
            push(buf.at[0, 0, a_from, pl.ds(lo, n)], buf.at[0, 0, a_to, pl.ds(lo, n)], send_2.at[i], recv_2.at[i], along_2(d))

        def wait_2nd(a, g):
            lo, n = GROUPS[g]
            landed(buf.at[0, 0, a, pl.ds(lo, n)], recv_2.at[n2 + (a - 1) * 2 + g])

        def send_3rd(b_from, b_to, a, g, d):
            lo, n = GROUPS[g]
            i = n3 + ((b_to - 1) * 4 + a) * 2 + g
            push(buf.at[0, b_from, a, pl.ds(lo, n)], buf.at[0, b_to, a, pl.ds(lo, n)], send_3.at[i], recv_3.at[i], along_3(d))

        def wait_3rd(b, a, g):
            lo, n = GROUPS[g]
            landed(buf.at[0, b, a, pl.ds(lo, n)], recv_3.at[n3 + ((b - 1) * 4 + a) * 2 + g])

        def share(b, a, g):
            lo, n = GROUPS[g]
            i = 32 * ids + (b * 4 + a) * 2 + g
            push(buf.at[0, b, a, pl.ds(lo, n)], buf.at[1, b, a, pl.ds(lo, n)], send_p.at[i], recv_p.at[i], chip(flip=True))

        def shared(b, a, g):
            lo, n = GROUPS[g]
            landed(buf.at[1, b, a, pl.ds(lo, n)], recv_p.at[32 * ids + (b * 4 + a) * 2 + g])

        def onward(a, g):
            send_3rd(0, 1, a, g, 1)
            send_3rd(0, 2, a, g, -1)
            share(0, a, g)

        def plane():
            for g in range(2):
                wait_z(g)
                send_2nd(0, 1, g, 1)
                send_2nd(0, 2, g, -1)
                onward(0, g)
            for g in range(2):
                wait_2nd(1, g)
                if g == 0:
                    send_2nd(1, 3, g, 1)
                onward(1, g)
                wait_2nd(2, g)
                if g == 1:
                    send_2nd(2, 3, g, -1)
                onward(2, g)
            for g in range(2):
                wait_2nd(3, g)
                onward(3, g)

        def near(a):
            for g in range(2):
                wait_3rd(1, a, g)
                if g == 0:
                    send_3rd(1, 3, a, g, 1)
                share(1, a, g)
                wait_3rd(2, a, g)
                if g == 1:
                    send_3rd(2, 3, a, g, -1)
                share(2, a, g)

        def far(a):
            for g in range(2):
                wait_3rd(3, a, g)
                share(3, a, g)

        def partner(b, a):
            for g in range(2):
                shared(b, a, g)

        return go_z, plane, near, far, partner

    go_z, plane, near, far, partner = spread(0, wbuf, wpiece)
    go_z()
    wbuf[0, 0, 0, 0] = wpiece[...]
    for k in range(1, 8):
        slot = SLOT_OF[-STEPS[k]]
        push(bundle, bbuf.at[0, slot], send_bz.at[k - 1], recv_bz.at[slot - 1], chip(dz=STEPS[k]))
    bbuf[0, 0] = bundle[...]
    plane()
    for k in range(1, 8):
        landed(bbuf.at[0, k], recv_bz.at[k - 1])
    for d, a in ((1, 1), (-1, 2)):
        push(bbuf.at[0], bbuf.at[a], send_bx.at[a - 1], recv_bx.at[a - 1], chip(dx=d))
    for a in range(4):
        near(a)
    for a in range(4):
        far(a)
    landed(bbuf.at[1], recv_bx.at[0])
    push(bbuf.at[1, pl.ds(0, 4)], bbuf.at[3, pl.ds(0, 4)], send_bx.at[2], recv_bx.at[2], chip(dx=1))
    landed(bbuf.at[2], recv_bx.at[1])
    push(bbuf.at[2, pl.ds(4, 4)], bbuf.at[3, pl.ds(4, 4)], send_bx.at[3], recv_bx.at[3], chip(dx=-1))
    for b in range(4):
        for a in range(4):
            partner(b, a)
    landed(bbuf.at[3, pl.ds(0, 4)], recv_bx.at[2])
    landed(bbuf.at[3, pl.ds(4, 4)], recv_bx.at[3])

    lane32 = lax.broadcasted_iota(jnp.int32, (1, 4, 1, 128), 3) // 32
    quarter = (lane32 == lax.broadcasted_iota(jnp.int32, (1, 4, 1, 128), 1)).astype(F32)[0]

    def arrange(s, carry):
        kz = slot8((s // 4 - z + 8) % 8)
        kx = slot4((s % 4 - x + 4) % 4)
        for half, first in ((0, c), (1, 1 - c)):
            for u in range(2):
                rows = []
                for yy in range(4):
                    ky = slot4((yy - y + 4) % 4)
                    b, a = (ky, kx) if half == 0 else (kx, ky)
                    rows.append(wbuf[first, b, a, kz, u].astype(F32))
                w_down[pl.ds(pl.multiple_of(s * 32, 32), 32), pl.ds((2 * half + u) * 128, 128)] = jnp.concatenate(
                    rows, axis=0
                ).astype(BF16)
        r = bbuf[kx, kz, 4].astype(F32)
        r = (r[None] * quarter).reshape(32, 128)
        w_rot[pl.ds(pl.multiple_of(s * 32, 32), 32), :] = r.astype(BF16)
        o = bbuf[kx, kz, pl.ds(5, 4)].astype(F32).reshape(32, 128)
        w_out[pl.ds(pl.multiple_of(s * 32, 32), 32), :] = o.astype(BF16)
        return carry

    lax.fori_loop(0, 32, arrange, 0)

    def arrange_up(s, carry):
        kz = slot8((s // 2 - z + 8) % 8)
        halves = [slot4((2 * (s % 2) + i - x + 4) % 4) for i in range(2)]
        at = pl.ds(pl.multiple_of(s * 16, 16), 16)
        for u in range(2):
            pair = [bbuf[kx, kz, u].astype(F32) for kx in halves]
            w_uq[at, pl.ds(u * 128, 128)] = jnp.concatenate(pair, axis=0).astype(BF16)
        w_uk[at, :] = jnp.concatenate([bbuf[kx, kz, 2].astype(F32) for kx in halves], axis=0)
        w_uv[at, :] = jnp.concatenate([bbuf[kx, kz, 3].astype(F32) for kx in halves], axis=0)
        return carry

    lax.fori_loop(0, 16, arrange_up, 0)

    own = tok[...]
    down = nn(own, w_down[...])

    def normed(v, gain):
        v = v.astype(BF16).astype(F32)
        return v * lax.rsqrt(jnp.mean(v * v, axis=-1, keepdims=True) + EPS) * gain

    latent_q = normed(down[:, :256], query_gain[...]).astype(BF16)
    latent_k = normed(down[:, 256:], key_gain[...]).astype(BF16)
    r = nn(own, w_rot[...])
    r = (r + pltpu.roll(r, 64, 1))
    r = (r + pltpu.roll(r, 32, 1)).astype(BF16).astype(F32)
    r = r * cos_k[...] + pltpu.roll(r, 16, 1) * sin_k[...]
    lane = lax.broadcasted_iota(jnp.int32, (16, 128), 1)
    in_a = lane < 32
    in_b = (lane >= 64) & (lane < 96)
    tail = jnp.where(in_a, r[:16], jnp.where(in_b, r[16:], kdoc[...])).astype(BF16)
    kbuf[0, 0, 0, 0, pl.ds(0, 32)] = latent_k[:, :128]
    kbuf[0, 0, 0, 0, pl.ds(32, 32)] = latent_k[:, 128:]
    kbuf[0, 0, 0, 0, pl.ds(64, 16)] = tail
    qlbuf[pl.ds(tp, 1)] = latent_q[None]

    go_z, plane, near, far, partner = spread(1, kbuf, kbuf.at[0, 0, 0, 0])
    go_z()
    for i, (dy, flip) in enumerate(tp_peers):
        push(qlbuf.at[tp], qlbuf.at[tp], send_t.at[i], recv_t.at[i], chip(dy=dy, flip=flip))

    lane = lax.broadcasted_iota(jnp.int32, (256, 128), 1)
    uk = w_uk[...]
    head0 = jnp.where(lane < 64, uk, 0.0).astype(BF16)
    head1 = jnp.where(lane < 64, pltpu.roll(uk, 64, 1), 0.0).astype(BF16)
    row = lax.broadcasted_iota(jnp.int32, (128, 128), 0)
    col = lax.broadcasted_iota(jnp.int32, (128, 128), 1)
    for g in range(2):
        pick = ((row - 64 * g == col - 64) & (col >= 64) & (col < 96)).astype(F32).astype(BF16)
        kx_w[g, pl.ds(0, 256), pl.ds(0, 128)] = head0
        kx_w[g, pl.ds(0, 256), pl.ds(128, 128)] = head1
        kx_w[g, pl.ds(256, 128), pl.ds(0, 128)] = pick
        kx_w[g, pl.ds(256, 128), pl.ds(128, 128)] = pick
    vt_w[...] = jnp.transpose(w_uv[...]).astype(BF16)
    top[...] = jnp.full_like(top, UNSEEN)
    total[...] = jnp.zeros_like(total)
    acc[...] = jnp.zeros_like(acc)

    plane()

    for i, (dy, flip) in enumerate(tp_peers):
        source = ((y + 4 - dy) % 4) * 2 + (1 - c if flip else c)
        landed(qlbuf.at[source], recv_t.at[i])
    q = nn(qlbuf[...].reshape(256, 256), w_uq[...]).astype(BF16).astype(F32)
    for h in range(2):
        v = q[:, 128 * h : 128 * h + 128]
        qx[h] = (v * cos_q[...] + pltpu.roll(v, 96, 1) * sin_q[...]).astype(BF16)

    row = lax.broadcasted_iota(jnp.int32, (128, 256), 0)
    doc_pick = [(row == 64 * g + 32).astype(F32).astype(BF16) for g in range(2)]

    def unit(side, b, a):
        block = kbuf[side, b, a]
        keys, docs, values = [], [], []
        for g in range(2):
            low = block[:, 16 * g : 16 * g + 16].reshape(128, 128)
            high = block[:, 32 + 16 * g : 48 + 16 * g].reshape(128, 128)
            rest = block[:, 64:80].reshape(128, 128)
            latent = jnp.concatenate([low, high], axis=1)
            keys.append(nn(jnp.concatenate([latent, rest], axis=1), kx_w[g]).astype(BF16))
            docs.append(nn(rest, doc_pick[g]))
            values.append(nt(vt_w[...], latent).astype(BF16))
        keys = jnp.concatenate(keys, axis=0)
        values = jnp.concatenate(values, axis=1)
        same = jnp.concatenate(docs, axis=0) == qdoc[...]
        for h in range(2):
            s = nt(keys[:, 128 * h : 128 * h + 128], qx[h])
            s = jnp.where(same, s, MASKED)
            old = top[h]
            new = jnp.maximum(old, jnp.max(s, axis=0, keepdims=True))
            p = jnp.exp2(s * SCALE_2 - new * SCALE_2)
            fade = jnp.exp2((old - new) * SCALE_2)
            top[h] = new
            total[h] = total[h] * fade + jnp.sum(p, axis=0, keepdims=True)
            acc[h] = acc[h] * fade + nn(values[64 * h : 64 * h + 64], p.astype(BF16))

    def units(count, place):
        def one(i, carry):
            unit(*place(i))
            return carry

        lax.fori_loop(0, count, one, 0)

    for a in range(4):
        partner(0, a)
    units(8, lambda i: (i // 4, 0, i % 4))
    for a in range(4):
        near(a)
        partner(1, a)
        partner(2, a)
        units(4, lambda i: (i // 2, 1 + i % 2, a))
    for a in range(4):
        far(a)
        partner(3, a)
        units(2, lambda i: (i, 3, a))

    rows = []
    for h in range(2):
        rows.append(acc[h] / total[h])
    attended = jnp.transpose(jnp.concatenate(rows, axis=0)).astype(BF16)
    logs = [top[h] * SCALE + jnp.log(total[h]) for h in range(2)]
    logs = jnp.transpose(jnp.concatenate(logs + [jnp.zeros((126, 256), F32)], axis=0))
    log_sums[...] = logs[:, 0:2]
    summed = nt(attended, w_out[...]).astype(BF16)
    partial[...] = summed.reshape(8, 32, 1024)
    for i, (dy, flip) in enumerate(tp_peers):
        target = ((y + dy) % 4) * 2 + (1 - c if flip else c)
        push(partial.at[target], rsbuf.at[i], send_t.at[7 + i], recv_t.at[7 + i], chip(dy=dy, flip=flip))
    out = partial[pl.ds(tp, 1)][0].astype(F32)
    for i in range(7):
        landed(rsbuf.at[i], recv_t.at[7 + i])
        out = out + rsbuf[i].astype(F32)
    mixed[...] = normed(out, out_gain[...]).astype(BF16)
    for copy in started:
        copy.wait_send()


def local(
    tokens,
    doc_ids,
    down_query,
    down_key,
    down_rotary,
    query_gain,
    key_gain,
    up_query,
    up_key,
    up_value,
    output_weight,
    out_gain,
):
    sp = lax.axis_index("sp")
    tp = lax.axis_index("tp")
    y, c = tp // 2, tp % 2
    half = jnp.where(c == 0, down_query, down_key)
    wpiece = lax.dynamic_slice_in_dim(half, 8 * y, 8, 0).reshape(8, 2, 128).transpose(1, 0, 2)
    uq = up_query.reshape(8, 2, 96)
    uq = jnp.concatenate([uq, uq[..., 80:96], uq[..., 64:80]], axis=-1).transpose(1, 0, 2)
    rot = down_rotary.reshape(4, 8, 32).transpose(1, 0, 2).reshape(1, 8, 128)
    wo = output_weight.T.reshape(4, 8, 128)
    bundle = jnp.concatenate([uq, up_key[None], up_value[None], rot, wo], axis=0)
    docs = doc_ids.astype(F32)
    own_docs = lax.dynamic_slice_in_dim(docs, 32 * tp, 32, 0)
    lane = jnp.arange(128)
    kdoc = jnp.where(lane == 32, own_docs[:16, None], jnp.where(lane == 96, own_docs[16:, None], 0.0))
    inverse = THETA ** (-(lane % 16).astype(F32) / 16)
    positions = sp * 256 + jnp.arange(256, dtype=jnp.int32)
    angles = positions.astype(F32)[:, None] * inverse[None, :]
    cosine, sine = jnp.cos(angles), jnp.sin(angles)
    signed = jnp.where(lane % 32 < 16, -sine, sine)
    turned = (lane >= 64) & (lane < 96)
    cos_q = jnp.where(lane < 64, 1.0, jnp.where(turned, cosine, 0.0))
    sin_q = jnp.where(turned, signed, 0.0)
    cos_k = lax.dynamic_slice_in_dim(cosine, 32 * tp, 32, 0)
    sin_k = lax.dynamic_slice_in_dim(signed, 32 * tp, 32, 0)
    dma = pltpu.SemaphoreType.DMA
    vm = pltpu.VMEM
    mixed, log_sums = pl.pallas_call(
        body,
        out_shape=(jax.ShapeDtypeStruct((32, 1024), BF16), jax.ShapeDtypeStruct((256, 2), F32)),
        in_specs=[pl.BlockSpec(memory_space=pltpu.VMEM)] * 12,
        out_specs=(pl.BlockSpec(memory_space=pltpu.VMEM),) * 2,
        scratch_shapes=[
            vm((2, 4, 4, 8, 2, 8, 128), BF16),
            vm((4, 8, 9, 8, 128), BF16),
            vm((2, 4, 4, 8, 80, 128), BF16),
            vm((8, 32, 256), BF16),
            vm((1024, 512), BF16),
            vm((1024, 128), BF16),
            vm((256, 256), BF16),
            vm((256, 128), F32),
            vm((256, 128), F32),
            vm((1024, 128), BF16),
            vm((2, 384, 256), BF16),
            vm((128, 256), BF16),
            vm((2, 256, 128), BF16),
            vm((2, 1, 256), F32),
            vm((2, 1, 256), F32),
            vm((2, 64, 256), F32),
            vm((8, 32, 1024), BF16),
            vm((7, 32, 1024), BF16),
            dma((2, 7)),
            dma((2, 7)),
            dma((12,)),
            dma((12,)),
            dma((48,)),
            dma((48,)),
            dma((64,)),
            dma((64,)),
            dma((7,)),
            dma((7,)),
            dma((4,)),
            dma((4,)),
            dma((14,)),
            dma((14,)),
        ],
        compiler_params=pltpu.CompilerParams(
            collective_id=0, has_side_effects=True, vmem_limit_bytes=40 * 1024 * 1024
        ),
    )(
        tokens,
        wpiece,
        bundle,
        docs.reshape(1, 256),
        kdoc,
        cos_q,
        sin_q,
        cos_k,
        sin_k,
        query_gain.reshape(1, 256),
        key_gain.reshape(1, 256),
        out_gain.reshape(1, 1024),
    )
    return mixed, log_sums


def solution(mesh):
    both = ("sp", "tp")
    return jax.shard_map(
        local,
        mesh=mesh,
        in_specs=(
            P(both, None),
            P("sp"),
            P("sp", None),
            P("sp", None),
            P("sp", None),
            P(),
            P(),
            P("sp", "tp"),
            P("sp", "tp"),
            P("sp", "tp"),
            P("tp", "sp"),
            P(),
        ),
        out_specs=(P(both, None), P("sp", "tp")),
        check_vma=False,
    )
```

time: 403 us -> 110 us (0.27)
  blocking collectives: 260 us -> 0 us
  Pallas kernels: 0 us -> 103 us
  waiting for transfers between devices: 45.4 us -> 0 us
  local copies, waits for them, and re-layouts: 36.5 us -> 4.35 us
  matrix products: 27.4 us -> 0 us
  between operations: 14.4 us -> 0.8 us
  other arithmetic: 14 us -> 1.46 us
    all_gather x16 -> x0, blocking collectives: 260 us -> none  [the longest x15 224 us: whole_of(): value = lax.all_gather(value, axis, axis=dim, tiled=True)]
    pallas_call x0 -> x1, Pallas kernels: none -> 103 us  [local(): pl.pallas_call(body, out_shape=(jax.ShapeDtypeStruct((32, 1024), BF16), j...]
    reduce_scatter x1 -> x0, waiting for transfers between devices: 45.4 us -> none  [own_rows_2(): lax.psum_scatter(sent, axis, scatter_dimension=0, tiled=True)]
    squeeze x32 -> x0, local copies, waits for them, and re-layouts: 29.6 us -> none  [over_blocks(): carry, unused = lax.scan(advance, carry, pieces_split)]
    dot_general x103 -> x0, matrix products: 27.4 us -> none  [the longest x32 8.78 us: attend(): jnp.einsum('qhr,kr->hqk', query_turned, key_turned, preferred_element_typ...]
    reshape x3 -> x4, local copies, waits for them, and re-layouts: 5.87 us -> 0.18 us  [the longest x2 0.09 us: local(): rot = down_rotary.reshape(4, 8, 32).transpose(1, 0, 2).reshape(1, 8, 128)]
    reduce_sum x35 -> x0, other arithmetic: 5.14 us -> none  [the longest x32 3.96 us: attend(): weight_sum = weight_sum * rescale + jnp.sum(weights, axis=-1)]
  transfers between devices with their start and end apart: 2 -> 0, of which waited for: 1 -> 0; matrix products, arithmetic and copies ran while one was open for 0% -> 0% of each run, Pallas kernels for 0% -> 0%
where the time goes in v1:
time: 110 us
  Pallas kernels  103 us (94%)
  local copies, waits for them, and re-layouts  4.35 us (4%)
  other arithmetic  1.46 us (1%)
    pallas_call x1, Pallas kernels, local(): pl.pallas_call(body, out_shape=(jax.ShapeDtypeStruct((32, 1024), BF16), j...  103 us
    unnamed x24, local copies, waits for them, and re-layouts  3.26 us

profile of v1, /device:TPU:1, one launch (start us, length us, event | category | flops | bytes accessed | tf_op | source)
XLA Modules:
  0.0 109.8 jit_solution(17566489876833788268)
XLA Ops:
  0.7 0.7 fusion.wpiece
  1.4 0.0 copy-start.9
  1.4 0.7 copy-done.9
  2.1 0.1 dynamic_slice.13
  2.1 0.1 fusion.7
  2.2 0.1 select_select_fusion.1.kdoc
  2.3 0.6 negate_select_fusion
  2.9 0.0 copy-start.6
  2.9 0.0 copy-start.7
  2.9 0.0 copy-start.8
  2.9 0.0 copy-start.4
  3.0 0.0 copy-start
  3.0 0.6 copy-done.6
  3.6 0.1 reshape.52
  3.7 0.1 fusion.6
  3.8 0.1 constant_dynamic-update-slice_fusion.4
  3.8 0.0 copy-done.7
  3.8 0.0 copy-done.8
  3.9 0.0 copy-done.4
  3.9 0.0 copy-start.5
  3.9 0.1 reshape.54
  4.0 0.6 copy-done.5
  4.6 0.0 copy-start.3
  4.6 0.0 copy-start.1
  4.6 0.0 copy-start.2
  4.6 0.0 copy-done
  4.6 0.7 copy-done.3
  5.3 0.0 copy-done.1
  5.3 0.0 copy-done.2
  5.3 103.2 %shard_map.131 = (bf16[32,1024]{1,0:T(8,128)(2,1)S(1)}, f32[256,2]{1,0:T(8,128)S(1)}) custom-call(bf16[32,1024]{1,0:T(8,128)(2,1)S(1)} %copy-done, bf16[2,8,128]{2,1,0:T(8,128)(2,1)S(1)} %fusion.wpiece, bf16[9,8,128]{2,1,0:T(8,128)(2,1)S(1)} %constant_dynamic-update-slice_fusion.bundle, f32[1,256]{1,0:T(1,128)S(1)} %bitcast.25, ...), custom_call_target="tpu_custom_call" | custom-call | tf_op jit(solution)/shard_map/pallas_call | solution.py:444
  108.5 0.7 copy.20
  109.1 0.6 copy.28
  (14 shorter events, 0.1 us)
Async XLA Ops:
  1.4 0.7 copy-start.9
  2.9 0.7 copy-start.6
  2.9 0.9 copy-start.7
  2.9 0.9 copy-start.8
  2.9 0.9 copy-start.4
  3.0 1.6 %copy-start = (bf16[32,1024]{1,0:T(8,128)(2,1)S(1)}, bf16[32,1024]{1,0:T(8,128)(2,1)}, u32[]{:S(2)}) copy-start(bf16[32,1024]{1,0:T(8,128)(2,1)} %tok.1) | copy-start | bytes 196612
  3.9 0.7 copy-start.5
  4.6 0.7 copy-start.3
  4.6 0.7 copy-start.1
  4.6 0.7 copy-start.2

commit v2 on v1

--- a/solution.py
+++ b/solution.py
@@ -12,8 +12,8 @@
 ROPE = 32
 THETA = 10000.0
 EPS = 1e-06
-UNSEEN = -1e30
-MASKED = -3e38
+UNSEEN = -(2.0**97)
+APART = -(2.0**100)
 SCALE = 1.0 / math.sqrt(NOPE + ROPE)
 SCALE_2 = SCALE * math.log2(math.e)
 MESH = pl.DeviceIdType.MESH
@@ -292,9 +292,8 @@
     r = (r + pltpu.roll(r, 32, 1)).astype(BF16).astype(F32)
     r = r * cos_k[...] + pltpu.roll(r, 16, 1) * sin_k[...]
     lane = lax.broadcasted_iota(jnp.int32, (16, 128), 1)
-    in_a = lane < 32
-    in_b = (lane >= 64) & (lane < 96)
-    tail = jnp.where(in_a, r[:16], jnp.where(in_b, r[16:], kdoc[...])).astype(BF16)
+    turned = jnp.where(lane < 64, r[:16], r[16:])
+    tail = jnp.where(lane % 64 < 32, turned, kdoc[...]).astype(BF16)
     kbuf[0, 0, 0, 0, pl.ds(0, 32)] = latent_k[:, :128]
     kbuf[0, 0, 0, 0, pl.ds(32, 32)] = latent_k[:, 128:]
     kbuf[0, 0, 0, 0, pl.ds(64, 16)] = tail
@@ -312,7 +311,7 @@
     row = lax.broadcasted_iota(jnp.int32, (128, 128), 0)
     col = lax.broadcasted_iota(jnp.int32, (128, 128), 1)
     for g in range(2):
-        pick = ((row - 64 * g == col - 64) & (col >= 64) & (col < 96)).astype(F32).astype(BF16)
+        pick = ((row - 64 * g == col - 64) & (col >= 64)).astype(F32).astype(BF16)
         kx_w[g, pl.ds(0, 256), pl.ds(0, 128)] = head0
         kx_w[g, pl.ds(0, 256), pl.ds(128, 128)] = head1
         kx_w[g, pl.ds(256, 128), pl.ds(0, 128)] = pick
@@ -330,28 +329,21 @@
     q = nn(qlbuf[...].reshape(256, 256), w_uq[...]).astype(BF16).astype(F32)
     for h in range(2):
         v = q[:, 128 * h : 128 * h + 128]
-        qx[h] = (v * cos_q[...] + pltpu.roll(v, 96, 1) * sin_q[...]).astype(BF16)
-
-    row = lax.broadcasted_iota(jnp.int32, (128, 256), 0)
-    doc_pick = [(row == 64 * g + 32).astype(F32).astype(BF16) for g in range(2)]
-
-    def unit(side, b, a):
-        block = kbuf[side, b, a]
-        keys, docs, values = [], [], []
+        qx[h] = (v * cos_q[...] + pltpu.roll(v, 96, 1) * sin_q[...] + qdoc[...]).astype(BF16)
+
+    def unit(side, b):
+        block = kbuf[side, b]
+        keys, values = [], []
         for g in range(2):
-            low = block[:, 16 * g : 16 * g + 16].reshape(128, 128)
-            high = block[:, 32 + 16 * g : 48 + 16 * g].reshape(128, 128)
-            rest = block[:, 64:80].reshape(128, 128)
-            latent = jnp.concatenate([low, high], axis=1)
-            keys.append(nn(jnp.concatenate([latent, rest], axis=1), kx_w[g]).astype(BF16))
-            docs.append(nn(rest, doc_pick[g]))
-            values.append(nt(vt_w[...], latent).astype(BF16))
+            low = block[:, :, 16 * g : 16 * g + 16].reshape(512, 128)
+            high = block[:, :, 32 + 16 * g : 48 + 16 * g].reshape(512, 128)
+            rest = block[:, :, 64:80].reshape(512, 128)
+            keys.append(nn(jnp.concatenate([low, high, rest], axis=1), kx_w[g]).astype(BF16))
+            values.append(nt(vt_w[...], jnp.concatenate([low, high], axis=1)).astype(BF16))
         keys = jnp.concatenate(keys, axis=0)
         values = jnp.concatenate(values, axis=1)
-        same = jnp.concatenate(docs, axis=0) == qdoc[...]
         for h in range(2):
             s = nt(keys[:, 128 * h : 128 * h + 128], qx[h])
-            s = jnp.where(same, s, MASKED)
             old = top[h]
             new = jnp.maximum(old, jnp.max(s, axis=0, keepdims=True))
             p = jnp.exp2(s * SCALE_2 - new * SCALE_2)
@@ -360,25 +352,27 @@
             total[h] = total[h] * fade + jnp.sum(p, axis=0, keepdims=True)
             acc[h] = acc[h] * fade + nn(values[64 * h : 64 * h + 64], p.astype(BF16))
 
-    def units(count, place):
+    def units(b):
         def one(i, carry):
-            unit(*place(i))
+            unit(i, b)
             return carry
 
-        lax.fori_loop(0, count, one, 0)
+        lax.fori_loop(0, 2, one, 0)
 
     for a in range(4):
         partner(0, a)
-    units(8, lambda i: (i // 4, 0, i % 4))
+    units(0)
     for a in range(4):
         near(a)
-        partner(1, a)
-        partner(2, a)
-        units(4, lambda i: (i // 2, 1 + i % 2, a))
+    for b in (1, 2):
+        for a in range(4):
+            partner(b, a)
+        units(b)
     for a in range(4):
         far(a)
+    for a in range(4):
         partner(3, a)
-        units(2, lambda i: (i, 3, a))
+    units(3)
 
     rows = []
     for h in range(2):
@@ -426,9 +420,11 @@
     wo = output_weight.T.reshape(4, 8, 128)
     bundle = jnp.concatenate([uq, up_key[None], up_value[None], rot, wo], axis=0)
     docs = doc_ids.astype(F32)
-    own_docs = lax.dynamic_slice_in_dim(docs, 32 * tp, 32, 0)
     lane = jnp.arange(128)
-    kdoc = jnp.where(lane == 32, own_docs[:16, None], jnp.where(lane == 96, own_docs[16:, None], 0.0))
+    seen = docs[:, None] == (lane % 32).astype(F32)[None, :]
+    qdoc = jnp.where(lane >= 96, jnp.where(seen, 0.0, APART), 0.0)
+    own = lax.dynamic_slice_in_dim(seen, 32 * tp, 32, 0)
+    kdoc = jnp.where(lane < 64, own[:16], own[16:]).astype(F32)
     inverse = THETA ** (-(lane % 16).astype(F32) / 16)
     positions = sp * 256 + jnp.arange(256, dtype=jnp.int32)
     angles = positions.astype(F32)[:, None] * inverse[None, :]
@@ -487,7 +483,7 @@
         tokens,
         wpiece,
         bundle,
-        docs.reshape(1, 256),
+        qdoc,
         kdoc,
         cos_q,
         sin_q,

time: 110 us -> 92.2 us (0.84)
  Pallas kernels: 103 us -> 84 us
  local copies, waits for them, and re-layouts: 4.35 us -> 5.55 us
    pallas_call x1, Pallas kernels: 103 us -> 84 us  [local(): pl.pallas_call(body, out_shape=(jax.ShapeDtypeStruct((32, 1024), BF16), j...]
    unnamed x24, local copies, waits for them, and re-layouts: 3.26 us -> 4.61 us
where the time goes in v2:
time: 92.2 us; the launch traced here: 91.9 us
  Pallas kernels  84 us (91%)
  local copies, waits for them, and re-layouts  5.55 us (6%)
  other arithmetic  1.61 us (2%)
    pallas_call x1, Pallas kernels, local(): pl.pallas_call(body, out_shape=(jax.ShapeDtypeStruct((32, 1024), BF16), j...  84 us
    unnamed x24, local copies, waits for them, and re-layouts  4.61 us

profile of v2, /device:TPU:1, one launch (start us, length us, event | category | flops | bytes accessed | tf_op | source)
XLA Modules:
  0.0 91.9 jit_solution(13073802071981578888)
XLA Ops:
  0.7 0.7 fusion.1.wpiece
  1.4 0.0 copy-start.9
  1.4 0.7 copy-done.9
  2.1 0.1 broadcast_compare_fusion
  2.3 0.6 negate_select_fusion
  2.8 0.0 copy-start.6
  2.9 0.7 copy-done.6
  3.5 0.1 reshape.58
  3.6 0.1 fusion.7
  3.7 0.0 copy-start.7
  3.7 0.0 copy-start.8
  3.7 0.1 constant_dynamic-update-slice_fusion.4
  3.8 0.6 copy-done.7
  4.4 0.0 copy-start.4
  4.4 0.0 copy-done.8
  4.4 0.7 copy-done.4
  5.1 0.0 copy-start.5
  5.1 0.1 reshape.60
  5.2 0.6 copy-done.5
  5.8 0.0 copy-start
  5.8 0.0 copy-start.3
  5.8 0.1 select_select_fusion.1.qdoc
  5.9 0.0 copy-start.1
  5.9 0.0 copy-start.2
  5.9 0.7 copy-done
  6.6 0.0 copy-done.3
  6.6 0.0 copy-done.1
  6.6 0.0 copy-done.2
  6.6 84.0 %shard_map.131 = (bf16[32,1024]{1,0:T(8,128)(2,1)S(1)}, f32[256,2]{1,0:T(8,128)S(1)}) custom-call(bf16[32,1024]{1,0:T(8,128)(2,1)S(1)} %copy-done, bf16[2,8,128]{2,1,0:T(8,128)(2,1)S(1)} %fusion.1.wpiece, bf16[9,8,128]{2,1,0:T(8,128)(2,1)S(1)} %constant_dynamic-update-slice_fusion.bundle, f32[256,128]{1,0:T(8,128)S(1)} %select_select_fusion.1.qdoc, ...), custom_call_target="tpu_custom_call" | custom-call | tf_op jit(solution)/shard_map/pallas_call | solution.py:440
  90.6 0.7 copy.20
  91.3 0.6 copy.28
  (16 shorter events, 0.1 us)
Async XLA Ops:
  1.4 0.7 copy-start.9
  2.8 0.7 copy-start.6
  3.7 0.7 copy-start.7
  3.7 0.7 copy-start.8
  4.4 0.7 copy-start.4
  5.1 0.7 copy-start.5
  5.8 0.8 copy-start
  5.8 0.8 copy-start.3
  5.9 0.7 copy-start.1
  5.9 0.7 copy-start.2

commit v3 on v2

v3 whole, which is shorter than its diff:
```python
import functools
import math

import jax
import jax.numpy as jnp
from jax import lax
from jax.experimental import pallas as pl
from jax.experimental.pallas import tpu as pltpu
from jax.sharding import PartitionSpec as P

NOPE = 64
ROPE = 32
THETA = 10000.0
EPS = 1e-06
UNSEEN = -(2.0**97)
NOTHING = -1e30
APART = -(2.0**100)
SCALE = 1.0 / math.sqrt(NOPE + ROPE)
SCALE_2 = SCALE * math.log2(math.e)
MESH = pl.DeviceIdType.MESH
F32 = jnp.float32
BF16 = jnp.bfloat16

STEPS = (0, 1, -1, 2, -2, 3, -3, 4)
SLOT_OF = {0: 0, 1: 1, -1: 2, 2: 3, -2: 4, 3: 5, -3: 6, 4: 7, -4: 7}


K_GROUPS = ((0, 1), (1, 4), (5, 3))


def slot8(r):
    late = r // 5
    return (1 - late) * (2 * r - 1 + (8 - r) // 8) + late * (16 - 2 * r)


def slot4(r):
    return 2 * r - r // 2 - 4 * (r // 3)


def nt(a, b):
    return lax.dot_general(a, b, (((1,), (1,)), ((), ())), preferred_element_type=F32)


def nn(a, b):
    return jnp.dot(a, b, preferred_element_type=F32)


def body(
    tok,
    wpiece,
    rot,
    up,
    out_w,
    qdoc,
    kdoc,
    cos_q,
    sin_q,
    cos_k,
    sin_k,
    query_gain,
    key_gain,
    out_gain,
    mixed,
    log_sums,
    wbuf,
    rbuf,
    ubuf,
    obuf,
    kbuf,
    qlbuf,
    w_down,
    w_rot,
    w_uq,
    w_uk,
    w_uv,
    w_out,
    vt_w,
    qx,
    vt,
    top,
    total,
    acc,
    lbuf,
    shares,
    part_out,
    part_in,
    half_out,
    half_in,
    send_w,
    recv_w,
    send_r,
    recv_r,
    send_k,
    recv_k,
    send_t,
    recv_t,
):
    sp = lax.axis_index("sp")
    tp = lax.axis_index("tp")
    z, x = sp // 4, sp % 4
    y, c = tp // 2, tp % 2

    def chip(dz=0, dx=0, dy=0, flip=False):
        core = 1 - c if flip else c
        return (((z + dz + 8) % 8) * 4 + (x + dx + 4) % 4, ((y + dy + 4) % 4) * 2 + core)

    def along_2(d):
        return chip(dx=(1 - c) * d, dy=c * d)

    def along_3(d):
        return chip(dx=c * d, dy=(1 - c) * d)

    tp_peers = [(dy, flip) for dy in (1, 3, 2, 0) for flip in (False, True) if (dy, flip) != (0, False)]
    ring = ((1, 1), (2, -1), (3, 2))

    barrier = pltpu.get_barrier_semaphore()
    peers = [chip(dz=d) for d in STEPS[1:]] + [chip(dx=d) for _, d in ring]
    peers += [chip(dy=dy, flip=flip) for dy, flip in tp_peers]
    for peer in peers:
        pl.semaphore_signal(barrier, inc=1, device_id=peer, device_id_type=MESH)
    pl.semaphore_wait(barrier, len(peers))

    started = []

    def push(src, dst, ssem, rsem, peer):
        copy = pltpu.make_async_remote_copy(
            src_ref=src, dst_ref=dst, send_sem=ssem, recv_sem=rsem, device_id=peer, device_id_type=MESH
        )
        copy.start()
        started.append(copy)

    def landed(dst, rsem):
        pltpu.make_async_remote_copy(
            src_ref=dst, dst_ref=dst, send_sem=rsem, recv_sem=rsem, device_id=chip(flip=True), device_id_type=MESH
        ).wait_recv()

    def wide_z(i, buf, first):
        for k in range(1, 8):
            slot = SLOT_OF[-STEPS[k]]
            push(first, buf.at[0, 0, slot], send_w.at[i, k - 1], recv_w.at[i, slot - 1], chip(dz=STEPS[k]))

    def wide_2(i, buf):
        for k in range(1, 8):
            landed(buf.at[0, 0, k], recv_w.at[i, k - 1])
        for a, d in ring:
            push(buf.at[0, 0], buf.at[0, a], send_w.at[i, 6 + a], recv_w.at[i, 6 + a], along_2(d))

    def wide_3(i, buf):
        for a, d in ring:
            landed(buf.at[0, a], recv_w.at[i, 6 + a])
        for b, d in ring:
            push(buf.at[0], buf.at[b], send_w.at[i, 9 + b], recv_w.at[i, 9 + b], along_3(d))

    def wide_end(i, buf, b):
        landed(buf.at[b], recv_w.at[i, 9 + b])

    wbuf[0, 0, 0, 0] = wpiece[...]
    rbuf[0, 0] = rot[...]
    ubuf[0, 0, 0] = up[...]
    obuf[0, 0, 0] = out_w[...]
    ours, theirs = wbuf.at[0], wbuf.at[1]

    def share(i, at):
        push(at(ours), at(theirs), send_w.at[3, i], recv_w.at[3, i], chip(flip=True))

    wide_z(0, ours, wpiece)
    for a, d in ring:
        push(rot, rbuf.at[0, a], send_r.at[a - 1], recv_r.at[a - 1], chip(dx=d))
    wide_z(1, ubuf, up)
    wide_z(2, obuf, out_w)
    wide_2(0, ours)
    share(0, lambda w: w.at[0, 0])
    for a, d in ring:
        landed(rbuf.at[0, a], recv_r.at[a - 1])
    for k in range(1, 8):
        slot = SLOT_OF[-STEPS[k]]
        push(rbuf.at[0], rbuf.at[slot], send_r.at[2 + k], recv_r.at[2 + slot], chip(dz=STEPS[k]))
    wide_3(0, ours)
    share(1, lambda w: w.at[0, pl.ds(1, 3)])
    wide_2(1, ubuf)
    wide_2(2, obuf)
    for b in range(1, 4):
        wide_end(0, ours, b)
        share(1 + b, lambda w: w.at[b])
    wide_3(1, ubuf)
    for k in range(1, 8):
        landed(rbuf.at[k], recv_r.at[2 + k])
    landed(theirs.at[0, 0], recv_w.at[3, 0])
    landed(theirs.at[0, pl.ds(1, 3)], recv_w.at[3, 1])
    for b in range(1, 4):
        landed(theirs.at[b], recv_w.at[3, 1 + b])

    lane32 = lax.broadcasted_iota(jnp.int32, (1, 4, 1, 128), 3) // 32
    quarter = (lane32 == lax.broadcasted_iota(jnp.int32, (1, 4, 1, 128), 1)).astype(F32)[0]

    def slot_x(v):
        return slot4((v - x + 4) % 4)

    def slot_y(v):
        return slot4((v - y + 4) % 4)

    def arrange(s, carry):
        kz = slot8((s // 4 - z + 8) % 8)
        kx = slot_x(s % 4)
        for half, first in ((0, c), (1, 1 - c)):
            for u in range(2):
                rows = []
                for yy in range(4):
                    ky = slot_y(yy)
                    b, a = (ky, kx) if half == 0 else (kx, ky)
                    rows.append(wbuf[first, b, a, kz, u].astype(F32))
                w_down[pl.ds(pl.multiple_of(s * 32, 32), 32), pl.ds((2 * half + u) * 128, 128)] = jnp.concatenate(
                    rows, axis=0
                ).astype(BF16)
        r = rbuf[kz, kx].astype(F32)
        r = (r[None] * quarter).reshape(32, 128)
        w_rot[pl.ds(pl.multiple_of(s * 32, 32), 32), :] = r.astype(BF16)
        return carry

    lax.fori_loop(0, 32, arrange, 0)

    own = tok[...]
    down = nn(own, w_down[...])

    def normed(v, gain):
        v = v.astype(BF16).astype(F32)
        return v * lax.rsqrt(jnp.mean(v * v, axis=-1, keepdims=True) + EPS) * gain

    latent_q = normed(down[:, :256], query_gain[...]).astype(BF16)
    latent_k = normed(down[:, 256:], key_gain[...]).astype(BF16)
    r = nn(own, w_rot[...])
    r = r + pltpu.roll(r, 64, 1)
    r = (r + pltpu.roll(r, 32, 1)).astype(BF16).astype(F32)
    r = r * cos_k[...] + pltpu.roll(r, 16, 1) * sin_k[...]
    lane = lax.broadcasted_iota(jnp.int32, (16, 128), 1)
    turned = jnp.where(lane < 64, r[:16], r[16:])
    tail = jnp.where(lane % 64 < 32, turned, kdoc[...]).astype(BF16)
    kbuf[0, 0, 0, pl.ds(0, 32)] = latent_k[:, :128]
    kbuf[0, 0, 0, pl.ds(32, 32)] = latent_k[:, 128:]
    kbuf[0, 0, 0, pl.ds(64, 16)] = tail
    qlbuf[pl.ds(tp, 1)] = latent_q[None]

    def keys_x(g):
        lo, n = K_GROUPS[g]
        for k in range(max(lo, 1), lo + n):
            landed(kbuf.at[0, 0, k], recv_k.at[k - 1])
        run = pl.ds(lo, n)
        for a, d in ring:
            i = 7 + 3 * g + a - 1
            push(kbuf.at[0, 0, run], kbuf.at[0, a, run], send_k.at[i], recv_k.at[i], chip(dx=d))

    def keys_share(a):
        if a:
            for g, (lo, n) in enumerate(K_GROUPS):
                landed(kbuf.at[0, a, pl.ds(lo, n)], recv_k.at[7 + 3 * g + a - 1])
        push(kbuf.at[0, a], kbuf.at[1, a], send_k.at[16 + a], recv_k.at[16 + a], chip(flip=True))

    for k in range(1, 8):
        slot = SLOT_OF[-STEPS[k]]
        push(kbuf.at[0, 0, 0], kbuf.at[0, 0, slot], send_k.at[k - 1], recv_k.at[slot - 1], chip(dz=STEPS[k]))
    for i, (dy, flip) in enumerate(tp_peers):
        push(qlbuf.at[tp], qlbuf.at[tp], send_t.at[i], recv_t.at[i], chip(dy=dy, flip=flip))
    keys_x(0)
    for b in range(1, 4):
        wide_end(1, ubuf, b)

    def arrange_up(s, carry):
        kz = slot8((s // 2 - z + 8) % 8)
        at = pl.ds(pl.multiple_of(s * 16, 16), 16)
        for yy in range(4):
            ky = slot_y(yy)
            places = []
            for i in range(2):
                kx = slot_x(2 * (s % 2) + i)
                places.append(((1 - c) * ky + c * kx, (1 - c) * kx + c * ky))
            for u in range(4):
                v = jnp.concatenate([ubuf[b, a, kz, u].astype(F32) for b, a in places], axis=0)
                if u < 2:
                    w_uq[at, pl.ds((2 * yy + u) * 128, 128)] = v.astype(BF16)
                elif u == 2:
                    w_uk[yy, at, :] = v.astype(BF16)
                else:
                    w_uv[at, pl.ds(yy * 128, 128)] = v
        return carry

    def arrange_out(s, carry):
        kz = slot8((s // 4 - z + 8) % 8)
        kx = slot_x(s % 4)
        for yy in range(4):
            ky = slot_y(yy)
            o = obuf[(1 - c) * ky + c * kx, (1 - c) * kx + c * ky, kz].astype(F32).reshape(32, 128)
            w_out[pl.ds(pl.multiple_of(s * 32, 32), 32), pl.ds(yy * 128, 128)] = o.astype(BF16)
        return carry

    lax.fori_loop(0, 16, arrange_up, 0)
    vt_w[...] = jnp.transpose(w_uv[...]).astype(BF16)
    top[...] = jnp.full_like(top, UNSEEN)
    total[...] = jnp.zeros_like(total)
    acc[...] = jnp.zeros_like(acc)
    keys_x(1)

    for i, (dy, flip) in enumerate(tp_peers):
        source = ((y + 4 - dy) % 4) * 2 + (1 - c if flip else c)
        landed(qlbuf.at[source], recv_t.at[i])
    keys_x(2)
    keys_share(0)
    wide_3(2, obuf)
    lane = lax.broadcasted_iota(jnp.int32, (256, 128), 1)
    row = lax.broadcasted_iota(jnp.int32, (128, 128), 0)
    col = lax.broadcasted_iota(jnp.int32, (128, 128), 1)
    pick = [((row - 64 * g == col - 64) & (col >= 64)).astype(F32).astype(BF16) for g in range(2)]
    query_block = qlbuf[...].reshape(256, 256)

    def make_queries(yy, carry):
        for j in range(2):
            h = 2 * yy + j
            v = nn(query_block, w_uq[:, pl.ds(pl.multiple_of(h * 128, 128), 128)]).astype(BF16).astype(F32)
            rest = v * cos_q[...] + pltpu.roll(v, 96, 1) * sin_q[...] + qdoc[...]
            rest = jnp.where(lane < 64, 0.0, rest).astype(BF16)
            plain = jnp.where(lane < 64, v, 0.0)
            if j == 1:
                plain = pltpu.roll(plain, 64, 1)
            over = nt(w_uk[yy], plain.astype(BF16)).astype(BF16)
            for g in range(2):
                qx[g, h, pl.ds(0, 256)] = over
                qx[g, h, pl.ds(256, 128)] = nt(pick[g], rest).astype(BF16)
        return carry

    lax.fori_loop(0, 4, make_queries, 0)

    def attend(a):
        keys = []
        for g in range(2):
            low = kbuf[:, a, :, pl.ds(16 * g, 16)].reshape(256, 128)
            high = kbuf[:, a, :, pl.ds(32 + 16 * g, 16)].reshape(256, 128)
            rest = kbuf[:, a, :, pl.ds(64, 16)].reshape(256, 128)
            keys.append(jnp.concatenate([low, high, rest], axis=1))
            vt[:, pl.ds(256 * g, 256)] = nt(vt_w[...], keys[g][:, :256]).astype(BF16)

        def pair(i, carry):
            heads = [2 * i, 2 * i + 1]
            scores = [jnp.concatenate([nn(keys[g], qx[g, h]) for g in range(2)], axis=0) for h in heads]
            for h, s in zip(heads, scores):
                old = top[h]
                new = jnp.maximum(old, jnp.max(s, axis=0, keepdims=True))
                p = jnp.exp2(s * SCALE_2 - new * SCALE_2)
                fade = jnp.exp2((old - new) * SCALE_2)
                top[h] = new
                total[h] = total[h] * fade + jnp.sum(p, axis=0, keepdims=True)
                values = vt[pl.ds(pl.multiple_of(h * 64, 64), 64), :]
                acc[h] = acc[h] * fade + nn(values, p.astype(BF16))
            return carry

        lax.fori_loop(0, 4, pair, 0)

    landed(kbuf.at[1, 0], recv_k.at[16])
    attend(0)
    for a in range(1, 4):
        keys_share(a)
    for a in range(1, 4):
        landed(kbuf.at[1, a], recv_k.at[16 + a])
        attend(a)

    for h in range(8):
        seen = total[h] > 0.0
        lbuf[0, pl.ds(h, 1)] = jnp.where(seen, top[h] * SCALE_2 + jnp.log2(total[h]), NOTHING)
        acc[h] = acc[h] * jnp.where(seen, 1.0 / total[h], 0.0)
    for i, dy in ((1, 1), (2, 3), (3, 2)):
        push(lbuf.at[0], lbuf.at[i], send_t.at[6 + i], recv_t.at[6 + i], chip(dy=dy))
    part_out[...] = jnp.transpose(acc[...].reshape(512, 256)).astype(BF16).reshape(4, 64, 512)
    for i, dy in ((1, 1), (2, 3), (3, 2)):
        push(part_out.at[(y + dy) % 4], part_in.at[i - 1], send_t.at[9 + i], recv_t.at[9 + i], chip(dy=dy))
    for b in range(1, 4):
        wide_end(2, obuf, b)
    lax.fori_loop(0, 32, arrange_out, 0)
    for i in range(1, 4):
        landed(lbuf.at[i], recv_t.at[6 + i])
    logs = [lbuf[i] for i in range(4)]
    most = functools.reduce(jnp.maximum, logs)
    logs = [jnp.exp2(v - most) for v in logs]
    whole = sum(logs[1:], logs[0])
    logs = [v / whole for v in logs] + [(most + jnp.log2(whole)) * math.log(2.0)]
    flat = jnp.transpose(jnp.concatenate(logs + [jnp.zeros((88, 256), F32)], axis=0))
    shares[...] = flat.reshape(4, 64, 128)
    sums = [jnp.sum(jnp.where(lane == 32 + 2 * y + j, flat, 0.0), axis=1, keepdims=True) for j in range(2)]
    log_sums[...] = jnp.where(lane[:, 0:2] == 0, sums[0], sums[1])
    mine = shares[pl.ds(y, 1)][0]
    high = mine.astype(BF16)
    low = (mine - high.astype(F32)).astype(BF16)
    row = lax.broadcasted_iota(jnp.int32, (128, 512), 0)
    col = lax.broadcasted_iota(jnp.int32, (128, 512), 1)
    attended = jnp.zeros((64, 512), F32)
    for i in range(4):
        wide = (row == 8 * i + col // 64).astype(F32).astype(BF16)
        if i:
            landed(part_in.at[i - 1], recv_t.at[9 + i])
            part = part_in[i - 1]
        else:
            part = part_out[pl.ds(y, 1)][0]
        attended = attended + (nn(high, wide) + nn(low, wide)) * part.astype(F32)
    half_out[...] = nt(attended.astype(BF16), w_out[...]).reshape(2, 32, 1024).astype(BF16)
    push(half_out.at[1 - c], half_in, send_t.at[13], recv_t.at[13], chip(flip=True))
    out = half_out[pl.ds(c, 1)][0].astype(F32)
    landed(half_in, recv_t.at[13])
    mixed[...] = normed(out + half_in[...].astype(F32), out_gain[...]).astype(BF16)
    for copy in started:
        copy.wait_send()


def local(
    tokens,
    doc_ids,
    down_query,
    down_key,
    down_rotary,
    query_gain,
    key_gain,
    up_query,
    up_key,
    up_value,
    output_weight,
    out_gain,
):
    sp = lax.axis_index("sp")
    tp = lax.axis_index("tp")
    y, c = tp // 2, tp % 2
    half = jnp.where(c == 0, down_query, down_key)
    wpiece = lax.dynamic_slice_in_dim(half, 8 * y, 8, 0).reshape(8, 2, 128).transpose(1, 0, 2)
    uq = up_query.reshape(8, 2, 96)
    uq = jnp.concatenate([uq, uq[..., 80:96], uq[..., 64:80]], axis=-1).transpose(1, 0, 2)
    rot = down_rotary.reshape(4, 8, 32).transpose(1, 0, 2).reshape(8, 128)
    wo = output_weight.T.reshape(4, 8, 128)
    up = jnp.concatenate([uq, up_key[None], up_value[None]], axis=0)
    docs = doc_ids.astype(F32)
    lane = jnp.arange(128)
    seen = docs[:, None] == (lane % 32).astype(F32)[None, :]
    qdoc = jnp.where(lane >= 96, jnp.where(seen, 0.0, APART), 0.0)
    own = lax.dynamic_slice_in_dim(seen, 32 * tp, 32, 0)
    kdoc = jnp.where(lane < 64, own[:16], own[16:]).astype(F32)
    inverse = THETA ** (-(lane % 16).astype(F32) / 16)
    positions = sp * 256 + jnp.arange(256, dtype=jnp.int32)
    angles = positions.astype(F32)[:, None] * inverse[None, :]
    cosine, sine = jnp.cos(angles), jnp.sin(angles)
    signed = jnp.where(lane % 32 < 16, -sine, sine)
    turned = (lane >= 64) & (lane < 96)
    cos_q = jnp.where(lane < 64, 1.0, jnp.where(turned, cosine, 0.0))
    sin_q = jnp.where(turned, signed, 0.0)
    cos_k = lax.dynamic_slice_in_dim(cosine, 32 * tp, 32, 0)
    sin_k = lax.dynamic_slice_in_dim(signed, 32 * tp, 32, 0)
    dma = pltpu.SemaphoreType.DMA
    vm = pltpu.VMEM
    mixed, log_sums = pl.pallas_call(
        body,
        out_shape=(jax.ShapeDtypeStruct((32, 1024), BF16), jax.ShapeDtypeStruct((256, 2), F32)),
        in_specs=[pl.BlockSpec(memory_space=pltpu.VMEM)] * 14,
        out_specs=(pl.BlockSpec(memory_space=pltpu.VMEM),) * 2,
        scratch_shapes=[
            vm((2, 4, 4, 8, 2, 8, 128), BF16),
            vm((8, 4, 8, 128), BF16),
            vm((4, 4, 8, 4, 8, 128), BF16),
            vm((4, 4, 8, 4, 8, 128), BF16),
            vm((2, 4, 8, 80, 128), BF16),
            vm((8, 32, 256), BF16),
            vm((1024, 512), BF16),
            vm((1024, 128), BF16),
            vm((256, 1024), BF16),
            vm((4, 256, 128), BF16),
            vm((256, 512), F32),
            vm((1024, 512), BF16),
            vm((512, 256), BF16),
            vm((2, 8, 384, 256), BF16),
            vm((512, 512), BF16),
            vm((8, 1, 256), F32),
            vm((8, 1, 256), F32),
            vm((8, 64, 256), F32),
            vm((4, 8, 256), F32),
            vm((4, 64, 128), F32),
            vm((4, 64, 512), BF16),
            vm((3, 64, 512), BF16),
            vm((2, 32, 1024), BF16),
            vm((32, 1024), BF16),
            dma((4, 13)),
            dma((4, 13)),
            dma((10,)),
            dma((10,)),
            dma((20,)),
            dma((20,)),
            dma((14,)),
            dma((14,)),
        ],
        compiler_params=pltpu.CompilerParams(
            collective_id=0, has_side_effects=True, vmem_limit_bytes=40 * 1024 * 1024
        ),
    )(
        tokens,
        wpiece,
        rot,
        up,
        wo,
        qdoc,
        kdoc,
        cos_q,
        sin_q,
        cos_k,
        sin_k,
        query_gain.reshape(1, 256),
        key_gain.reshape(1, 256),
        out_gain.reshape(1, 1024),
    )
    return mixed, log_sums


def solution(mesh):
    both = ("sp", "tp")
    return jax.shard_map(
        local,
        mesh=mesh,
        in_specs=(
            P(both, None),
            P("sp"),
            P("sp", None),
            P("sp", None),
            P("sp", None),
            P(),
            P(),
            P("sp", "tp"),
            P("sp", "tp"),
            P("sp", "tp"),
            P("tp", "sp"),
            P(),
        ),
        out_specs=(P(both, None), P("sp", "tp")),
        check_vma=False,
    )
```

time: 92.2 us -> 73.1 us (0.79)
  Pallas kernels: 84 us -> 65.5 us
    pallas_call x1, Pallas kernels: 84 us -> 65.5 us  [local(): pl.pallas_call(body, out_shape=(jax.ShapeDtypeStruct((32, 1024), BF16), j...]
    unnamed x24 -> x21, local copies, waits for them, and re-layouts: 4.61 us -> 3.96 us
where the time goes in v3:
time: 73.1 us; the launch traced here: 72.8 us
  Pallas kernels  65.5 us (90%)
  local copies, waits for them, and re-layouts  4.88 us (7%)
  other arithmetic  1.61 us (2%)
  between operations  0.78 us (1%)
    pallas_call x1, Pallas kernels, local(): pl.pallas_call(body, out_shape=(jax.ShapeDtypeStruct((32, 1024), BF16), j...  65.5 us
    unnamed x21, local copies, waits for them, and re-layouts  3.96 us

profile of v3, /device:TPU:1, one launch (start us, length us, event | category | flops | bytes accessed | tf_op | source)
XLA Modules:
  0.0 72.8 jit_solution(11973605574673101988)
XLA Ops:
  0.7 0.7 fusion.1.wpiece
  1.4 0.0 copy-start.9
  1.4 0.7 copy-done.9
  2.1 0.1 broadcast_compare_fusion
  2.3 0.6 negate_select_fusion
  2.8 0.0 copy-start.6
  2.9 0.7 copy-done.6
  3.5 0.1 reshape.60
  3.6 0.1 fusion.7
  3.7 0.0 copy-start.8
  3.7 0.1 maximum_bitcast_fusion
  3.8 0.0 copy-start.7
  3.8 0.6 copy-done.8
  4.4 0.1 copy-done.7
  4.5 0.0 copy-start.5
  4.5 0.0 copy-start
  4.5 0.1 select_select_fusion.1.qdoc
  4.6 0.6 copy-done.5
  5.2 0.0 copy-start.1
  5.2 0.0 copy-start.4
  5.2 0.1 reshape.59.rot
  5.3 0.0 copy-start.2
  5.3 0.0 copy-start.3
  5.3 0.1 copy-done
  5.3 0.6 copy-done.1
  5.9 0.0 copy-done.4
  5.9 0.1 copy-done.2
  6.0 0.0 copy-done.3
  6.0 65.5 %shard_map.131 = (bf16[32,1024]{1,0:T(8,128)(2,1)S(1)}, f32[256,2]{1,0:T(8,128)S(1)}) custom-call(bf16[32,1024]{1,0:T(8,128)(2,1)S(1)} %copy-done, bf16[2,8,128]{2,1,0:T(8,128)(2,1)S(1)} %fusion.1.wpiece, bf16[8,128]{1,0:T(8,128)(2,1)S(1)} %reshape.59.rot, bf16[4,8,128]{2,1,0:T(8,128)(2,1)S(1)} %pad_maximum_fusion.up, bf16[4,8,128]{2,1,0:T(8,128)(2,1)S(1)} %bitcast.18, ...), custom_call_target="tpu_custom_call" | custom-call | tf_op jit(solution)/shard_map/pallas_call | solution.py:452
  71.5 0.7 copy.20
  72.2 0.6 copy.24
  (13 shorter events, 0.1 us)
Async XLA Ops:
  1.4 0.7 copy-start.9
  2.8 0.7 copy-start.6
  3.7 0.7 copy-start.8
  3.8 0.7 copy-start.7
  4.5 0.7 copy-start.5
  4.5 0.8 %copy-start = (bf16[32,1024]{1,0:T(8,128)(2,1)S(1)}, bf16[32,1024]{1,0:T(8,128)(2,1)}, u32[]{:S(2)}) copy-start(bf16[32,1024]{1,0:T(8,128)(2,1)} %tok.1) | copy-start | bytes 196612
  5.2 0.7 copy-start.1
  5.2 0.7 copy-start.4
  5.3 0.7 copy-start.2
  5.3 0.7 copy-start.3

commit v4 on v3

--- a/solution.py
+++ b/solution.py
@@ -3,6 +3,7 @@
 
 import jax
 import jax.numpy as jnp
+import numpy as np
 from jax import lax
 from jax.experimental import pallas as pl
 from jax.experimental.pallas import tpu as pltpu
@@ -12,6 +13,7 @@
 ROPE = 32
 THETA = 10000.0
 EPS = 1e-06
+INVERSE = [float(v) for v in np.float32(THETA) ** (-np.arange(16, dtype=np.float32) / 16)]
 UNSEEN = -(2.0**97)
 NOTHING = -1e30
 APART = -(2.0**100)
@@ -46,22 +48,31 @@
 
 
 def body(
-    tok,
-    wpiece,
-    rot,
-    up,
-    out_w,
-    qdoc,
-    kdoc,
-    cos_q,
-    sin_q,
-    cos_k,
-    sin_k,
+    tokens,
+    down_query,
+    down_key,
+    down_rotary,
+    up_query,
+    up_key,
+    up_value,
+    output_weight,
     query_gain,
     key_gain,
     out_gain,
+    doc_ids,
     mixed,
     log_sums,
+    tok,
+    rot_in,
+    up_in,
+    gain_q,
+    gain_k,
+    gain_o,
+    docs,
+    doc,
+    qdoc,
+    cosine,
+    sine,
     wbuf,
     rbuf,
     ubuf,
@@ -80,6 +91,10 @@
     top,
     total,
     acc,
+    scores_a,
+    scores_b,
+    highest_a,
+    highest_b,
     lbuf,
     shares,
     part_out,
@@ -94,6 +109,7 @@
     recv_k,
     send_t,
     recv_t,
+    fetch,
 ):
     sp = lax.axis_index("sp")
     tp = lax.axis_index("tp")
@@ -118,6 +134,43 @@
     peers += [chip(dy=dy, flip=flip) for dy, flip in tp_peers]
     for peer in peers:
         pl.semaphore_signal(barrier, inc=1, device_id=peer, device_id_type=MESH)
+
+    def fetched(i, src, dst):
+        copy = pltpu.make_async_copy(src, dst, fetch.at[i])
+        copy.start()
+        return copy
+
+    for core, weight in ((0, down_query), (1, down_key)):
+
+        @pl.when(c == core)
+        def _(weight=weight):
+            for u in range(2):
+                at = (pl.ds(pl.multiple_of(8 * y, 8), 8), pl.ds(128 * u, 128))
+                fetched(u, weight.at[at], wbuf.at[0, 0, 0, 0, u])
+
+    pairs = ((down_rotary, rot_in), (up_query, up_in), (up_key, ubuf.at[0, 0, 0, 2]))
+    pairs += tuple((output_weight.at[pl.ds(8 * i, 8)], obuf.at[0, 0, 0, i]) for i in range(4))
+    pairs += ((up_value, ubuf.at[0, 0, 0, 3]), (tokens, tok), (query_gain, gain_q), (key_gain, gain_k))
+    pairs += ((out_gain, gain_o), (doc_ids, docs))
+    copies = [fetched(2 + i, src, dst) for i, (src, dst) in enumerate(pairs)]
+    for copy in copies[:2]:
+        copy.wait()
+    lane = lax.broadcasted_iota(jnp.int32, (8, 128), 1)
+    row = lax.broadcasted_iota(jnp.int32, (32, 128), 0)
+    col = lax.broadcasted_iota(jnp.int32, (32, 128), 1)
+    r = nn(rot_in[...], (row == col % 32).astype(F32).astype(BF16))
+    r = [jnp.where(lane // 32 == g, r[8 * g : 8 * g + 8], 0.0) for g in range(4)]
+    rbuf[0, 0] = (r[0] + r[1] + r[2] + r[3]).astype(BF16)
+    u0 = up_in[:, 0:128].astype(F32)
+    u1 = jnp.concatenate([up_in[:, 128:192].astype(F32), jnp.zeros((8, 64), F32)], axis=1)
+    u1 = jnp.where(lane < 32, pltpu.roll(u0, 32, 1), pltpu.roll(u1, 32, 1))
+    for j, u in enumerate((u0, u1)):
+        u = jnp.where(lane < 96, u, jnp.where(lane < 112, pltpu.roll(u, 16, 1), pltpu.roll(u, 48, 1)))
+        ubuf[0, 0, 0, j] = u.astype(BF16)
+    for i in range(2):
+        pltpu.make_async_copy(wbuf.at[0, 0, 0, 0, i], wbuf.at[0, 0, 0, 0, i], fetch.at[i]).wait()
+    for copy in copies[2:]:
+        copy.wait()
     pl.semaphore_wait(barrier, len(peers))
 
     started = []
@@ -134,7 +187,8 @@
             src_ref=dst, dst_ref=dst, send_sem=rsem, recv_sem=rsem, device_id=chip(flip=True), device_id_type=MESH
         ).wait_recv()
 
-    def wide_z(i, buf, first):
+    def wide_z(i, buf):
+        first = buf.at[0, 0, 0]
         for k in range(1, 8):
             slot = SLOT_OF[-STEPS[k]]
             push(first, buf.at[0, 0, slot], send_w.at[i, k - 1], recv_w.at[i, slot - 1], chip(dz=STEPS[k]))
@@ -154,20 +208,30 @@
     def wide_end(i, buf, b):
         landed(buf.at[b], recv_w.at[i, 9 + b])
 
-    wbuf[0, 0, 0, 0] = wpiece[...]
-    rbuf[0, 0] = rot[...]
-    ubuf[0, 0, 0] = up[...]
-    obuf[0, 0, 0] = out_w[...]
     ours, theirs = wbuf.at[0], wbuf.at[1]
 
     def share(i, at):
         push(at(ours), at(theirs), send_w.at[3, i], recv_w.at[3, i], chip(flip=True))
 
-    wide_z(0, ours, wpiece)
+    wide_z(0, ours)
     for a, d in ring:
-        push(rot, rbuf.at[0, a], send_r.at[a - 1], recv_r.at[a - 1], chip(dx=d))
-    wide_z(1, ubuf, up)
-    wide_z(2, obuf, out_w)
+        push(rbuf.at[0, 0], rbuf.at[0, a], send_r.at[a - 1], recv_r.at[a - 1], chip(dx=d))
+    wide_z(1, ubuf)
+    wide_z(2, obuf)
+
+    lane = lax.broadcasted_iota(jnp.int32, (1, 128), 1) % 16
+    inverse = sum(jnp.where(lane == i, v, 0.0) for i, v in enumerate(INVERSE))
+    angles = (sp * 256 + lax.broadcasted_iota(jnp.int32, (256, 128), 0)).astype(F32) * inverse
+    lane = lax.broadcasted_iota(jnp.int32, (256, 128), 1)
+    cosine[...] = jnp.cos(angles).reshape(8, 32, 128)
+    sine[...] = (jnp.where(lane % 32 < 16, -1.0, 1.0) * jnp.sin(angles)).reshape(8, 32, 128)
+    for i in range(2):
+        turned = jnp.transpose(jnp.broadcast_to(docs[i : i + 1, :].astype(F32), (128, 128)))
+        doc[pl.ds(4 * i, 4)] = turned.reshape(4, 32, 128)
+    lane = lax.broadcasted_iota(jnp.int32, (256, 128), 1)
+    apart = jnp.where(doc[...].reshape(256, 128) == (lane - 96).astype(F32), 0.0, APART)
+    qdoc[...] = jnp.where(lane < 96, 0.0, apart)
+
     wide_2(0, ours)
     share(0, lambda w: w.at[0, 0])
     for a, d in ring:
@@ -226,15 +290,17 @@
         v = v.astype(BF16).astype(F32)
         return v * lax.rsqrt(jnp.mean(v * v, axis=-1, keepdims=True) + EPS) * gain
 
-    latent_q = normed(down[:, :256], query_gain[...]).astype(BF16)
-    latent_k = normed(down[:, 256:], key_gain[...]).astype(BF16)
+    latent_q = normed(down[:, :256], gain_q[...]).astype(BF16)
+    latent_k = normed(down[:, 256:], gain_k[...]).astype(BF16)
     r = nn(own, w_rot[...])
     r = r + pltpu.roll(r, 64, 1)
     r = (r + pltpu.roll(r, 32, 1)).astype(BF16).astype(F32)
-    r = r * cos_k[...] + pltpu.roll(r, 16, 1) * sin_k[...]
+    r = r * cosine[pl.ds(tp, 1)][0] + pltpu.roll(r, 16, 1) * sine[pl.ds(tp, 1)][0]
     lane = lax.broadcasted_iota(jnp.int32, (16, 128), 1)
     turned = jnp.where(lane < 64, r[:16], r[16:])
-    tail = jnp.where(lane % 64 < 32, turned, kdoc[...]).astype(BF16)
+    d = doc[pl.ds(tp, 1)][0]
+    d = jnp.where(lane < 64, d[:16], d[16:]) == (lane % 32).astype(F32)
+    tail = jnp.where(lane % 64 < 32, turned, d.astype(F32)).astype(BF16)
     kbuf[0, 0, 0, pl.ds(0, 32)] = latent_k[:, :128]
     kbuf[0, 0, 0, pl.ds(32, 32)] = latent_k[:, 128:]
     kbuf[0, 0, 0, pl.ds(64, 16)] = tail
@@ -315,12 +381,13 @@
         for j in range(2):
             h = 2 * yy + j
             v = nn(query_block, w_uq[:, pl.ds(pl.multiple_of(h * 128, 128), 128)]).astype(BF16).astype(F32)
-            rest = v * cos_q[...] + pltpu.roll(v, 96, 1) * sin_q[...] + qdoc[...]
-            rest = jnp.where(lane < 64, 0.0, rest).astype(BF16)
+            turned = v * cosine[...].reshape(256, 128) + pltpu.roll(v, 96, 1) * sine[...].reshape(256, 128)
+            turned = turned.astype(BF16).astype(F32) * SCALE_2
+            rest = jnp.where((lane < 64) | (lane >= 96), qdoc[...], turned).astype(BF16)
             plain = jnp.where(lane < 64, v, 0.0)
             if j == 1:
                 plain = pltpu.roll(plain, 64, 1)
-            over = nt(w_uk[yy], plain.astype(BF16)).astype(BF16)
+            over = (nt(w_uk[yy], plain.astype(BF16)) * SCALE_2).astype(BF16)
             for g in range(2):
                 qx[g, h, pl.ds(0, 256)] = over
                 qx[g, h, pl.ds(256, 128)] = nt(pick[g], rest).astype(BF16)
@@ -328,30 +395,44 @@
 
     lax.fori_loop(0, 4, make_queries, 0)
 
+    def keys_of(a, g):
+        low = kbuf[:, a, :, pl.ds(16 * g, 16)].reshape(256, 128)
+        high = kbuf[:, a, :, pl.ds(32 + 16 * g, 16)].reshape(256, 128)
+        return low, high, kbuf[:, a, :, pl.ds(64, 16)].reshape(256, 128)
+
     def attend(a):
-        keys = []
         for g in range(2):
-            low = kbuf[:, a, :, pl.ds(16 * g, 16)].reshape(256, 128)
-            high = kbuf[:, a, :, pl.ds(32 + 16 * g, 16)].reshape(256, 128)
-            rest = kbuf[:, a, :, pl.ds(64, 16)].reshape(256, 128)
-            keys.append(jnp.concatenate([low, high, rest], axis=1))
-            vt[:, pl.ds(256 * g, 256)] = nt(vt_w[...], keys[g][:, :256]).astype(BF16)
+            vt[:, pl.ds(256 * g, 256)] = nt(vt_w[...], jnp.concatenate(keys_of(a, g)[:2], axis=1)).astype(BF16)
+
+        def score(h, scores, highest):
+            new = top[h]
+            for g in range(2):
+                s = nn(jnp.concatenate(keys_of(a, g), axis=1), qx[g, h])
+                scores[pl.ds(256 * g, 256), :] = s
+                new = jnp.maximum(new, jnp.max(s, axis=0, keepdims=True))
+            highest[...] = new
+
+        def weigh(h, scores, highest):
+            new = highest[...]
+            p = jnp.exp2(scores[...] - new)
+            fade = jnp.exp2(top[h] - new)
+            top[h] = new
+            total[h] = total[h] * fade + jnp.sum(p, axis=0, keepdims=True)
+            values = vt[pl.ds(64 * h if isinstance(h, int) else pl.multiple_of(h * 64, 64), 64), :]
+            acc[h] = acc[h] * fade + nn(values, p.astype(BF16))
 
         def pair(i, carry):
-            heads = [2 * i, 2 * i + 1]
-            scores = [jnp.concatenate([nn(keys[g], qx[g, h]) for g in range(2)], axis=0) for h in heads]
-            for h, s in zip(heads, scores):
-                old = top[h]
-                new = jnp.maximum(old, jnp.max(s, axis=0, keepdims=True))
-                p = jnp.exp2(s * SCALE_2 - new * SCALE_2)
-                fade = jnp.exp2((old - new) * SCALE_2)
-                top[h] = new
-                total[h] = total[h] * fade + jnp.sum(p, axis=0, keepdims=True)
-                values = vt[pl.ds(pl.multiple_of(h * 64, 64), 64), :]
-                acc[h] = acc[h] * fade + nn(values, p.astype(BF16))
+            score(2 * i + 1, scores_b, highest_b)
+            weigh(2 * i, scores_a, highest_a)
+            score(2 * i + 2, scores_a, highest_a)
+            weigh(2 * i + 1, scores_b, highest_b)
             return carry
 
-        lax.fori_loop(0, 4, pair, 0)
+        score(0, scores_a, highest_a)
+        lax.fori_loop(0, 3, pair, 0)
+        score(7, scores_b, highest_b)
+        weigh(6, scores_a, highest_a)
+        weigh(7, scores_b, highest_b)
 
     landed(kbuf.at[1, 0], recv_k.at[16])
     attend(0)
@@ -363,7 +444,7 @@
 
     for h in range(8):
         seen = total[h] > 0.0
-        lbuf[0, pl.ds(h, 1)] = jnp.where(seen, top[h] * SCALE_2 + jnp.log2(total[h]), NOTHING)
+        lbuf[0, pl.ds(h, 1)] = jnp.where(seen, top[h] + jnp.log2(total[h]), NOTHING)
         acc[h] = acc[h] * jnp.where(seen, 1.0 / total[h], 0.0)
     for i, dy in ((1, 1), (2, 3), (3, 2)):
         push(lbuf.at[0], lbuf.at[i], send_t.at[6 + i], recv_t.at[6 + i], chip(dy=dy))
@@ -379,11 +460,12 @@
     most = functools.reduce(jnp.maximum, logs)
     logs = [jnp.exp2(v - most) for v in logs]
     whole = sum(logs[1:], logs[0])
-    logs = [v / whole for v in logs] + [(most + jnp.log2(whole)) * math.log(2.0)]
-    flat = jnp.transpose(jnp.concatenate(logs + [jnp.zeros((88, 256), F32)], axis=0))
-    shares[...] = flat.reshape(4, 64, 128)
-    sums = [jnp.sum(jnp.where(lane == 32 + 2 * y + j, flat, 0.0), axis=1, keepdims=True) for j in range(2)]
-    log_sums[...] = jnp.where(lane[:, 0:2] == 0, sums[0], sums[1])
+    logs = [v / whole for v in logs]
+    row = lax.broadcasted_iota(jnp.int32, (8, 256), 0)
+    whole = (most + jnp.log2(whole)) * math.log(2.0)
+    for j in range(2):
+        log_sums[pl.ds(j, 1)] = jnp.sum(jnp.where(row == 2 * y + j, whole, 0.0), axis=0, keepdims=True)
+    shares[...] = jnp.transpose(jnp.concatenate(logs + [jnp.zeros((96, 256), F32)], axis=0)).reshape(4, 64, 128)
     mine = shares[pl.ds(y, 1)][0]
     high = mine.astype(BF16)
     low = (mine - high.astype(F32)).astype(BF16)
@@ -402,7 +484,7 @@
     push(half_out.at[1 - c], half_in, send_t.at[13], recv_t.at[13], chip(flip=True))
     out = half_out[pl.ds(c, 1)][0].astype(F32)
     landed(half_in, recv_t.at[13])
-    mixed[...] = normed(out + half_in[...].astype(F32), out_gain[...]).astype(BF16)
+    mixed[...] = normed(out + half_in[...].astype(F32), gain_o[...]).astype(BF16)
     for copy in started:
         copy.wait_send()
 
@@ -421,40 +503,25 @@
     output_weight,
     out_gain,
 ):
-    sp = lax.axis_index("sp")
-    tp = lax.axis_index("tp")
-    y, c = tp // 2, tp % 2
-    half = jnp.where(c == 0, down_query, down_key)
-    wpiece = lax.dynamic_slice_in_dim(half, 8 * y, 8, 0).reshape(8, 2, 128).transpose(1, 0, 2)
-    uq = up_query.reshape(8, 2, 96)
-    uq = jnp.concatenate([uq, uq[..., 80:96], uq[..., 64:80]], axis=-1).transpose(1, 0, 2)
-    rot = down_rotary.reshape(4, 8, 32).transpose(1, 0, 2).reshape(8, 128)
-    wo = output_weight.T.reshape(4, 8, 128)
-    up = jnp.concatenate([uq, up_key[None], up_value[None]], axis=0)
-    docs = doc_ids.astype(F32)
-    lane = jnp.arange(128)
-    seen = docs[:, None] == (lane % 32).astype(F32)[None, :]
-    qdoc = jnp.where(lane >= 96, jnp.where(seen, 0.0, APART), 0.0)
-    own = lax.dynamic_slice_in_dim(seen, 32 * tp, 32, 0)
-    kdoc = jnp.where(lane < 64, own[:16], own[16:]).astype(F32)
-    inverse = THETA ** (-(lane % 16).astype(F32) / 16)
-    positions = sp * 256 + jnp.arange(256, dtype=jnp.int32)
-    angles = positions.astype(F32)[:, None] * inverse[None, :]
-    cosine, sine = jnp.cos(angles), jnp.sin(angles)
-    signed = jnp.where(lane % 32 < 16, -sine, sine)
-    turned = (lane >= 64) & (lane < 96)
-    cos_q = jnp.where(lane < 64, 1.0, jnp.where(turned, cosine, 0.0))
-    sin_q = jnp.where(turned, signed, 0.0)
-    cos_k = lax.dynamic_slice_in_dim(cosine, 32 * tp, 32, 0)
-    sin_k = lax.dynamic_slice_in_dim(signed, 32 * tp, 32, 0)
     dma = pltpu.SemaphoreType.DMA
     vm = pltpu.VMEM
     mixed, log_sums = pl.pallas_call(
         body,
-        out_shape=(jax.ShapeDtypeStruct((32, 1024), BF16), jax.ShapeDtypeStruct((256, 2), F32)),
-        in_specs=[pl.BlockSpec(memory_space=pltpu.VMEM)] * 14,
+        out_shape=(jax.ShapeDtypeStruct((32, 1024), BF16), jax.ShapeDtypeStruct((2, 256), F32)),
+        in_specs=[pl.BlockSpec(memory_space=pltpu.HBM)] * 12,
         out_specs=(pl.BlockSpec(memory_space=pltpu.VMEM),) * 2,
         scratch_shapes=[
+            vm((32, 1024), BF16),
+            vm((32, 32), BF16),
+            vm((8, 192), BF16),
+            vm((1, 256), F32),
+            vm((1, 256), F32),
+            vm((1, 1024), F32),
+            vm((2, 128), jnp.int32),
+            vm((8, 32, 128), F32),
+            vm((256, 128), F32),
+            vm((8, 32, 128), F32),
+            vm((8, 32, 128), F32),
             vm((2, 4, 4, 8, 2, 8, 128), BF16),
             vm((8, 4, 8, 128), BF16),
             vm((4, 4, 8, 4, 8, 128), BF16),
@@ -473,6 +540,10 @@
             vm((8, 1, 256), F32),
             vm((8, 1, 256), F32),
             vm((8, 64, 256), F32),
+            vm((512, 256), F32),
+            vm((512, 256), F32),
+            vm((1, 256), F32),
+            vm((1, 256), F32),
             vm((4, 8, 256), F32),
             vm((4, 64, 128), F32),
             vm((4, 64, 512), BF16),
@@ -487,27 +558,26 @@
             dma((20,)),
             dma((14,)),
             dma((14,)),
+            dma((15,)),
         ],
         compiler_params=pltpu.CompilerParams(
-            collective_id=0, has_side_effects=True, vmem_limit_bytes=40 * 1024 * 1024
+            collective_id=0, has_side_effects=True, vmem_limit_bytes=62 * 1024 * 1024
         ),
     )(
         tokens,
-        wpiece,
-        rot,
-        up,
-        wo,
-        qdoc,
-        kdoc,
-        cos_q,
-        sin_q,
-        cos_k,
-        sin_k,
+        down_query,
+        down_key,
+        down_rotary,
+        up_query,
+        up_key,
+        up_value,
+        output_weight.T,
         query_gain.reshape(1, 256),
         key_gain.reshape(1, 256),
         out_gain.reshape(1, 1024),
+        doc_ids.reshape(2, 128),
     )
-    return mixed, log_sums
+    return mixed, log_sums.T
 
 
 def solution(mesh):

time: 73.1 us -> 67.4 us (0.922)
  local copies, waits for them, and re-layouts: 4.88 us -> 2.06 us
  other arithmetic: 1.61 us -> 0 us
  Pallas kernels: 65.5 us -> 64.5 us
    unnamed x21 -> x4, local copies, waits for them, and re-layouts: 3.96 us -> 2.06 us
    pallas_call x1, Pallas kernels: 65.5 us -> 64.5 us  [local(): pl.pallas_call(body, out_shape=(jax.ShapeDtypeStruct((32, 1024), BF16), j...]
    transpose x2 -> x0, other arithmetic: 0.79 us -> none  [the longest x1 0.71 us: local(): lax.dynamic_slice_in_dim(half, 8 * y, 8, 0).reshape(8, 2, 128)]
where the time goes in v4:
time: 67.4 us; the launch traced here: 67.2 us
  Pallas kernels  64.5 us (96%)
  local copies, waits for them, and re-layouts  2.06 us (3%)
    pallas_call x1, Pallas kernels, local(): pl.pallas_call(body, out_shape=(jax.ShapeDtypeStruct((32, 1024), BF16), j...  64.5 us
    unnamed x4, local copies, waits for them, and re-layouts  2.06 us

profile of v4, /device:TPU:1, one launch (start us, length us, event | category | flops | bytes accessed | tf_op | source)
XLA Modules:
  0.0 67.2 jit_solution(3602065946898233147)
XLA Ops:
  0.6 64.5 %shard_map.131 = (bf16[32,1024]{1,0:T(8,128)(2,1)}, f32[2,256]{1,0:T(2,128)}) custom-call(bf16[32,1024]{1,0:T(8,128)(2,1)} %tokens.1, bf16[32,256]{1,0:T(8,128)(2,1)} %down_query.1, bf16[32,256]{1,0:T(8,128)(2,1)} %down_key.1, bf16[32,32]{1,0:T(8,128)(2,1)} %down_rotary.1, bf16[8,192]{1,0:T(8,128)(2,1)} %up_query.1, bf16[8,128]{1,0:T(8,128)(2,1)} %up_key.1, ...), custom_call_target="tpu_custom_call" | custom-call | tf_op jit(solution)/shard_map/pallas_call | solution.py:508
  65.1 0.0 copy-start
  65.2 1.5 %copy.16 = bf16[32,1024]{1,0:T(8,128)(2,1)} copy(bf16[32,1024]{1,0:T(8,128)(2,1)} %get-tuple-element.8) | data formatting | bytes 131072
  66.6 0.0 copy-done
  66.6 0.6 copy.17
Async XLA Ops:
  65.1 1.5 %copy-start = (f32[2,256]{1,0:T(2,128)S(1)}, f32[2,256]{1,0:T(2,128)}, u32[]{:S(2)}) copy-start(f32[2,256]{1,0:T(2,128)} %get-tuple-element.5) | copy-start | bytes 6148
